TPU v7x, 32 devices: a whole 2x2x4 slice. The times are simulated.
32 devices in a mesh: st: 16 (over z, y, x), tp: 2 (over core).
Axes of the slice: x: 2, y: 2, z: 4, core: 2. Of those that a mesh axis runs over, the one named last changes fastest.
Arguments:
- tokens: bfloat16 [12288, 2048], P('st'), may hold values from -6 to 6, as said below
- route_ids: int32 [192, 4], P('st'), may hold values from 0 to 383, as said below
- store: bfloat16 [384, 128, 2048], P('st'), may hold values from -6 to 6, as said below
- token_gain: float32 [2048], replicated, may hold values from 0.1 to 1.9
- store_gain: float32 [2048], replicated, may hold values from 0.1 to 1.9
- carry_weight: bfloat16 [2048, 512], P(None, 'tp'), may hold values from -0.125 to 0.125
- spatial_weight: bfloat16 [2048, 512], P(None, 'tp'), may hold values from -0.125 to 0.125
- spatial_gain: float32 [512], P('tp'), may hold values from 0.1 to 1.9
- position_mix: bfloat16 [8, 128, 128], P('tp'), may hold values from -0.5 to 0.5
- position_bias: float32 [8, 128], P('tp'), may hold values from 0.1 to 1.9
- query_weight: bfloat16 [2048, 512], P(None, 'tp'), may hold values from -0.86178639 to 0.86178639, as said below
- key_weight: bfloat16 [2048, 512], P(None, 'tp'), may hold values from -0.86178639 to 0.86178639, as said below
- read_weight: bfloat16 [2048, 512], P(None, 'tp'), may hold values from -0.125 to 0.125
- blend_weight: bfloat16 [2048, 512], P(None, 'tp'), may hold values from -0.125 to 0.125
- output_weight: bfloat16 [512, 2048], replicated, may hold values from -0.25 to 0.25
Outputs:
- mixed: bfloat16 [12288, 2048], P(('st', 'tp'))
Inputs may be any that keep to these rules, and one draw needn't show every extreme that they name: `route_ids`: each entry is a passage index; passage p is held by index p // 24 of st. All entries of the spans of one index of st (aligned blocks of 12 rows) are different; they name at most 6 passage held by any one index of st, exactly 6 held by the index before their own (cyclically), and at least one held by the index half the axis away. `tokens`: Activations; in some draws the first token of some spans equals a row of a passage that the span reads. `store`: passage rows. `query_weight`: A projection matrix. `key_weight`: A projection matrix.
All inputs are finite; a program needn't handle non-finite values.
Results may differ from a plain program's by a relative error of at most 0.012.
The roundings to bfloat16 on the way count: a program that leaves them out, or rounds other values in their place, can miss the bound.
Values may be sent and summed in bfloat16 or wider, within the bound.
A program may use at most 128 MiB of HBM per device.

v0:
```python
import functools

import jax
import jax.numpy as jnp
from jax import lax
from jax.experimental import pallas as pl
from jax.experimental.pallas import tpu as pltpu
from jax.sharding import PartitionSpec as P

norm_eps = 1e-06
bf16 = jnp.bfloat16
f32 = jnp.float32


def normed_rows(matrix, gain):
    values = matrix.astype(f32)
    scaled = values * lax.rsqrt(jnp.mean(values * values, axis=-1, keepdims=True) + norm_eps)
    return (scaled * gain).astype(bf16)


def query_kernel(span_length, slots, slot_span, tok_ref, gain_ref, wq_ref, normed_ref, sent_ref, q_ref):
    step = pl.program_id(0)
    rows = tok_ref.shape[0]
    normed = normed_rows(tok_ref[...], gain_ref[...])
    normed_ref[...] = normed
    q = jnp.dot(normed, wq_ref[...], preferred_element_type=f32).astype(bf16)
    per = rows // span_length
    for s in range(per):
        q_ref[step * per + s] = q[s * span_length : (s + 1) * span_length]

    @pl.when(step == pl.num_programs(0) - 1)
    def _():
        def body(i, carry):
            sent_ref[i] = q_ref[slot_span[i]]
            return carry

        lax.fori_loop(0, slots, body, 0)


def store_kernel(st_ref, gain_ref, wk_ref, wv_ref, k_ref, vt_ref):
    count, length, _ = st_ref.shape
    for p in range(count):
        normed = normed_rows(st_ref[p], gain_ref[...])
        k_ref[p] = jnp.dot(normed, wk_ref[...], preferred_element_type=f32).astype(bf16)
        v = jnp.dot(normed, wv_ref[...], preferred_element_type=f32)
        vt_ref[p] = v.T.astype(bf16)


def attend(q, k, vt, heads):
    length, width = q.shape
    dim = width // heads
    row_head = lax.broadcasted_iota(jnp.int32, (heads * length, width), 0) // length
    lane_head = lax.broadcasted_iota(jnp.int32, (heads * length, width), 1) // dim
    stacked = jnp.where(row_head == lane_head, jnp.concatenate([q] * heads, axis=0), jnp.zeros((), bf16))
    s = lax.dot_general(k, stacked, (((1,), (1,)), ((), ())), preferred_element_type=f32) * dim ** (-0.5)
    peak = jnp.max(s, axis=0, keepdims=True)
    w = jnp.exp(s - peak)
    total = jnp.sum(w, axis=0, keepdims=True)
    o = jnp.dot(vt, w.astype(bf16), preferred_element_type=f32)
    col_head = lax.broadcasted_iota(jnp.int32, (dim, heads * length), 1) // length
    out = o[0:dim]
    for h in range(1, heads):
        out = jnp.where(col_head == h, o[h * dim : (h + 1) * dim], out)
    return (out / total).astype(bf16), peak + jnp.log(total)


def attention_kernel(heads, n, ids, q_ref, k_ref, vt_ref, val_ref, lev_ref, out_val, out_lev, send, recv):
    me = lax.axis_index("st")
    cap = q_ref.shape[1]

    barrier = pltpu.get_barrier_semaphore()

    def greet(d, carry):
        pl.semaphore_signal(
            barrier,
            inc=1,
            device_id={"st": lax.rem(me + d, n)},
            device_id_type=pl.DeviceIdType.MESH,
        )
        return carry

    lax.fori_loop(1, n, greet, 0)
    pl.semaphore_wait(barrier, n - 1)

    def compute(dst, val_to, lev_to):
        for c in range(cap):
            i = ids[dst * cap + c]
            val, lev = attend(q_ref[dst, c], k_ref[i], vt_ref[i], heads)
            val_to[dst, c] = val
            lev_to[dst, c : c + 1] = lev

    def copies(d):
        dst = lax.rem(me + d, n)
        pairs = ((out_val, val_ref), (out_lev, lev_ref))
        return [
            pltpu.make_async_remote_copy(
                src_ref=src.at[dst],
                dst_ref=to.at[me],
                send_sem=send.at[j, d],
                recv_sem=recv.at[j, d],
                device_id={"st": dst},
                device_id_type=pl.DeviceIdType.MESH,
            )
            for j, (src, to) in enumerate(pairs)
        ]

    def offset(i):
        j = n // 2 + i
        return j % n + j // n

    def launch(d):
        for copy in copies(d):
            copy.start()

    compute(lax.rem(me + offset(0), n), out_val, out_lev)

    def step(i, carry):
        compute(lax.rem(me + offset(i), n), out_val, out_lev)
        launch(offset(i - 1))
        return carry

    lax.fori_loop(1, n - 1, step, 0)
    compute(me, val_ref, lev_ref)
    launch(offset(n - 2))

    def finish(d, carry):
        for copy in copies(d):
            copy.wait()
        return carry

    lax.fori_loop(1, n, finish, 0)


def merge_kernel(heads, spans, picks, pos, val_ref, lev_ref, gated_ref, blend_ref, out_ref):
    step = pl.program_id(0)
    dim, width = val_ref.shape[1:]
    length = width // heads
    for s in range(spans):
        first = (step * spans + s) * picks
        levels = [lev_ref[pos[first + p]] for p in range(picks)]
        top = functools.reduce(jnp.maximum, levels)
        ws = [jnp.exp(lev - top) for lev in levels]
        total = sum(ws)
        summed = sum(w * val_ref[pos[first + p]].astype(f32) for p, w in enumerate(ws))
        mem = (summed / total).T
        mem = jnp.concatenate([mem[h * length : (h + 1) * length] for h in range(heads)], axis=1)
        rows = slice(s * length, (s + 1) * length)
        out_ref[rows] = (gated_ref[rows] + blend_ref[rows] * mem).astype(bf16)


def per_device(
    tokens,
    route_ids,
    store,
    token_gain,
    store_gain,
    carry_weight,
    spatial_weight,
    spatial_gain,
    position_mix,
    position_bias,
    query_weight,
    key_weight,
    read_weight,
    blend_weight,
    output_weight,
):
    row_count, model = tokens.shape
    local_heads, block_length = position_mix.shape[:2]
    width = carry_weight.shape[1]
    head_dim = width // local_heads
    span_count, pick_count = route_ids.shape
    span_length = row_count // span_count
    store_count, passage_length = store.shape[:2]
    owner_count = lax.axis_size("st")
    requests = span_count * pick_count
    cap = max(1, 2 * requests // owner_count)
    slots = owner_count * cap

    flat_ids = route_ids.reshape(requests)
    owner = flat_ids // store_count
    order = jnp.arange(requests, dtype=jnp.int32)
    earlier = (owner[:, None] == owner[None, :]) & (order[None, :] < order[:, None])
    position = owner * cap + jnp.sum(earlier.astype(jnp.int32), axis=1)
    hit = position[None, :] == jnp.arange(slots, dtype=jnp.int32)[:, None]
    slot_local = jnp.sum(jnp.where(hit, (flat_ids % store_count)[None, :], 0), axis=1)
    slot_span = jnp.sum(jnp.where(hit, (order // pick_count)[None, :], 0), axis=1)
    piece_local = lax.all_to_all(
        slot_local.reshape(owner_count, cap), "st", split_axis=0, concat_axis=0, tiled=True
    ).reshape(slots)

    tile = 2 * span_length
    normed, sent = pl.pallas_call(
        functools.partial(query_kernel, span_length, slots),
        grid_spec=pltpu.PrefetchScalarGridSpec(
            num_scalar_prefetch=1,
            grid=(row_count // tile,),
            in_specs=[
                pl.BlockSpec((tile, model), lambda i, _: (i, 0)),
                pl.BlockSpec((1, model), lambda i, _: (0, 0)),
                pl.BlockSpec((model, width), lambda i, _: (0, 0)),
            ],
            out_specs=[
                pl.BlockSpec((tile, model), lambda i, _: (i, 0)),
                pl.BlockSpec((slots, span_length, width), lambda i, _: (0, 0, 0)),
            ],
            scratch_shapes=[pltpu.VMEM((span_count, span_length, width), bf16)],
        ),
        out_shape=[
            jax.ShapeDtypeStruct((row_count, model), bf16),
            jax.ShapeDtypeStruct((slots, span_length, width), bf16),
        ],
        cost_estimate=pl.CostEstimate(
            flops=2 * row_count * model * width, bytes_accessed=4 * row_count * model, transcendentals=0
        ),
        name="query",
    )(slot_span, tokens, token_gain.reshape(1, model), query_weight)
    piece_q = lax.all_to_all(
        sent.reshape(owner_count, cap, span_length, width), "st", split_axis=0, concat_axis=0, tiled=True
    )

    group = 2
    keys, values_t = pl.pallas_call(
        store_kernel,
        grid=(store_count // group,),
        in_specs=[
            pl.BlockSpec((group, passage_length, model), lambda i: (i, 0, 0)),
            pl.BlockSpec((1, model), lambda i: (0, 0)),
            pl.BlockSpec((model, width), lambda i: (0, 0)),
            pl.BlockSpec((model, width), lambda i: (0, 0)),
        ],
        out_specs=[
            pl.BlockSpec((group, passage_length, width), lambda i: (i, 0, 0)),
            pl.BlockSpec((group, width, passage_length), lambda i: (i, 0, 0)),
        ],
        out_shape=[
            jax.ShapeDtypeStruct((store_count, passage_length, width), bf16),
            jax.ShapeDtypeStruct((store_count, width, passage_length), bf16),
        ],
        cost_estimate=pl.CostEstimate(
            flops=4 * store_count * passage_length * model * width,
            bytes_accessed=2 * store_count * passage_length * model,
            transcendentals=0,
        ),
        name="store",
    )(store, store_gain.reshape(1, model), key_weight, read_weight)

    carry_branch = jnp.dot(normed, carry_weight, preferred_element_type=f32)
    spatial = jax.nn.gelu(jnp.dot(normed, spatial_weight, preferred_element_type=f32), approximate=False)
    total_width = width * lax.axis_size("tp")
    moment_one, moment_two = lax.psum(
        (jnp.sum(spatial, axis=1), jnp.sum(spatial * spatial, axis=1)), "tp"
    )
    channel_mean = (moment_one / total_width)[:, None]
    channel_spread = (moment_two / total_width)[:, None] - channel_mean * channel_mean
    spatial_in = (
        (spatial - channel_mean) * lax.rsqrt(channel_spread + norm_eps) * spatial_gain
    ).astype(bf16)
    blocks = spatial_in.reshape(row_count // block_length, block_length, local_heads, head_dim)
    mixed_blocks = jnp.einsum("hij,njhc->nihc", position_mix, blocks, preferred_element_type=f32)
    mixed_blocks = mixed_blocks + position_bias.T[None, :, :, None]
    gated_mix = jax.nn.gelu(carry_branch, approximate=False) * mixed_blocks.reshape(row_count, width)
    blend_gate = jax.nn.sigmoid(jnp.dot(normed, blend_weight, preferred_element_type=f32))

    keys, gated_mix, blend_gate = lax.optimization_barrier((keys, gated_mix, blend_gate))
    value_shape = (owner_count, cap, head_dim, local_heads * span_length)
    level_shape = (owner_count, cap, local_heads * span_length)
    vmem = pl.BlockSpec(memory_space=pltpu.VMEM)
    back_values, back_levels = pl.pallas_call(
        functools.partial(attention_kernel, local_heads, owner_count),
        in_specs=[pl.BlockSpec(memory_space=pltpu.SMEM), vmem, vmem, vmem],
        out_specs=[vmem, vmem],
        out_shape=[jax.ShapeDtypeStruct(value_shape, bf16), jax.ShapeDtypeStruct(level_shape, f32)],
        scratch_shapes=[
            pltpu.VMEM(value_shape, bf16),
            pltpu.VMEM(level_shape, f32),
            pltpu.SemaphoreType.DMA((2, owner_count)),
            pltpu.SemaphoreType.DMA((2, owner_count)),
        ],
        compiler_params=pltpu.CompilerParams(collective_id=0, has_side_effects=True),
        name="attention",
    )(piece_local, piece_q, keys, values_t)

    spans = 4 if span_count % 4 == 0 else 1
    mixed_rows = pl.pallas_call(
        functools.partial(merge_kernel, local_heads, spans, pick_count),
        grid_spec=pltpu.PrefetchScalarGridSpec(
            num_scalar_prefetch=1,
            grid=(span_count // spans,),
            in_specs=[
                pl.BlockSpec((slots, head_dim, local_heads * span_length), lambda i, _: (0, 0, 0)),
                pl.BlockSpec((slots, 1, local_heads * span_length), lambda i, _: (0, 0, 0)),
                pl.BlockSpec((spans * span_length, width), lambda i, _: (i, 0)),
                pl.BlockSpec((spans * span_length, width), lambda i, _: (i, 0)),
            ],
            out_specs=pl.BlockSpec((spans * span_length, width), lambda i, _: (i, 0)),
        ),
        out_shape=jax.ShapeDtypeStruct((row_count, width), bf16),
        name="merge",
    )(
        position,
        back_values.reshape(slots, head_dim, local_heads * span_length),
        back_levels.reshape(slots, 1, local_heads * span_length),
        gated_mix,
        blend_gate,
    )
    by_rows = lax.all_to_all(mixed_rows, "tp", split_axis=0, concat_axis=1, tiled=True)
    return jnp.dot(by_rows, output_weight, preferred_element_type=f32).astype(bf16)


def solution(mesh):
    in_specs = (
        P("st", None),
        P("st", None),
        P("st", None, None),
        P(),
        P(),
        P(None, "tp"),
        P(None, "tp"),
        P("tp"),
        P("tp", None, None),
        P("tp", None),
        P(None, "tp"),
        P(None, "tp"),
        P(None, "tp"),
        P(None, "tp"),
        P(),
    )
    out_specs = P(("st", "tp"), None)
    return jax.shard_map(
        per_device, mesh=mesh, in_specs=in_specs, out_specs=out_specs, check_vma=False
    )
```

profile of v0, /device:TPU:0, one launch (start us, length us, event | category | flops | bytes accessed | tf_op | source)
XLA Modules:
  0.0 195.4 jit_solution(7383409042361852117)
XLA Ops:
  0.0 0.0 copy-start
  0.0 0.8 broadcast_remainder_fusion
  0.8 0.7 sign_compare_fusion
  1.5 0.1 copy.48
  1.6 0.1 div.36
  1.7 0.1 copy.47
  1.8 0.1 rem.39
  1.9 0.1 copy.46
  2.0 0.1 ne.74
  2.1 0.2 convert_reduce_fusion
  2.3 0.0 copy-start.3
  2.3 0.7 select_reduce_fusion
  3.0 0.7 all_to_all.23
  3.7 8.3 %all-to-all-start = ((s32[16,1,6]{2,1,0:T(1,128)}), s32[16,1,6]{2,1,0:T(1,128)S(1)}, u32[]{:S(2)}, u32[]{:S(2)}) async-start(s32[16,1,6]{2,1,0:T(1,128)} %bitcast), calls=%async_computation | async-start | bytes 16384 | tf_op jit(solution)/shard_map/all_to_all | solution.py:188
  12.0 9.2 %query.1 = (bf16[768,2048]{1,0:T(8,128)(2,1)}, bf16[96,64,256]{2,1,0:T(8,128)(2,1)}) custom-call(s32[96]{0:T(128)} %get-tuple-element.25.slot_span, bf16[768,2048]{1,0:T(8,128)(2,1)} %tok_ref.1, f32[1,2048]{1,0:T(1,128)} %bitcast.31, bf16[2048,256]{1,0:T(8,128)(2,1)} %wq_ref.1), custom_call_target="tpu_custom_call" | custom-call | flops 805306368 | bytes 6291456 | tf_op jit(solution)/shard_map/query/pallas_call | solution.py:193
  21.3 0.0 all-to-all-done
  21.3 0.0 copy-done.3
  21.3 7.0 %all-to-all-start.1 = ((bf16[16,6,64,256]{3,2,1,0:T(8,128)(2,1)}), bf16[16,6,64,256]{3,2,1,0:T(8,128)(2,1)}, u32[]{:S(2)}, u32[]{:S(2)}) async-start(bf16[16,6,64,256]{3,2,1,0:T(8,128)(2,1)} %bitcast.27), calls=%async_computation.1 | async-start | bytes 6291456 | tf_op jit(solution)/shard_map/all_to_all | solution.py:218
  28.2 0.0 copy-start.4
  28.3 0.0 copy-start.1
  28.3 0.0 copy-start.2
  28.3 4.9 %fusion.26 = (f32[768]{0:T(1024)S(1)}, f32[768]{0:T(1024)S(1)}, f32[768,256]{1,0:T(8,128)S(1)}) fusion(bf16[768,2048]{1,0:T(8,128)(2,1)} %get-tuple-element.16, bf16[2048,256]{1,0:T(8,128)(2,1)} %param.21), kind=kOutput, calls=%fused_computation.66 | convolution fusion | flops 818477568 | bytes 4986880 | tf_op jit(solution)/shard_map/dot_general | solution.py:249
  33.1 2.5 %all-reduce = (f32[768]{0:T(1024)S(1)}, f32[768]{0:T(1024)S(1)}) all-reduce(f32[768]{0:T(1024)S(1)} %get-tuple-element.24, f32[768]{0:T(1024)S(1)} %get-tuple-element.23), channel_id=1, replica_groups=mesh['st'=16,'tp'=2] {'tp'}, use_global_device_ids=true, to_apply=%region_6.7 | all-reduce | flops 1536 | bytes 12288 | tf_op jit(solution)/shard_map/psum | solution.py:251
  35.7 0.0 copy-done.4
  35.7 0.3 multiply_convert_fusion
  35.9 0.3 reshape.124
  36.3 0.0 copy-done.1
  36.3 0.0 copy-done.2
  36.3 1.3 fusion.1
  37.6 2.4 %copy.62 = f32[6,128,4,64]{3,2,1,0:T(4,128)} copy(f32[6,128,4,64]{1,3,0,2:T(8,128)} %fusion.1) | data formatting | bytes 1572864 | tf_op jit(solution)/shard_map/reshape | solution.py:262
  40.0 2.2 %reshape.125 = f32[768,256]{1,0:T(8,128)S(1)} reshape(f32[6,128,4,64]{3,2,1,0:T(4,128)} %copy.62) | data formatting | bytes 1572864 | tf_op jit(solution)/shard_map/reshape | solution.py:262
  42.2 4.1 %fusion.3.blend_ref = f32[768,256]{1,0:T(8,128)} fusion(bf16[768,2048]{1,0:T(8,128)(2,1)} %get-tuple-element.16, bf16[2048,256]{1,0:T(8,128)(2,1)} %param.28), kind=kOutput, calls=%fused_computation.6 | convolution fusion | flops 805896192 | bytes 4980736 | tf_op jit(solution)/shard_map/dot_general | solution.py:263
  46.3 15.8 %store.1 = (bf16[24,128,256]{2,1,0:T(8,128)(2,1)}, bf16[24,256,128]{2,1,0:T(8,128)(2,1)}) custom-call(bf16[24,128,2048]{2,1,0:T(8,128)(2,1)} %st_ref.1, f32[1,2048]{1,0:T(1,128)} %bitcast.33, bf16[2048,256]{1,0:T(8,128)(2,1)} %wk_ref.1, bf16[2048,256]{1,0:T(8,128)(2,1)} %wv_ref.1), custom_call_target="tpu_custom_call" | custom-call | flops 6442450944 | bytes 12582912 | tf_op jit(solution)/shard_map/store/pallas_call | solution.py:223
  62.1 5.6 %fusion.6.gated_ref = f32[768,256]{1,0:T(8,128)} fusion(f32[768,256]{1,0:T(8,128)S(1)} %reshape.125, bf16[768,2048]{1,0:T(8,128)(2,1)} %get-tuple-element.16, bf16[2048,256]{1,0:T(8,128)(2,1)} %param.20), kind=kOutput, calls=%fused_computation.11 | convolution fusion | flops 818085888 | bytes 5767168 | tf_op jit(solution)/shard_map/dot_general | solution.py:248
  67.7 0.5 broadcast.309
  68.2 0.6 reduce.3
  68.8 0.6 reshape.115.ids
  69.4 19.6 %all-to-all-done.1.q_ref = bf16[16,6,64,256]{3,2,1,0:T(8,128)(2,1)} async-done(((bf16[16,6,64,256]{3,2,1,0:T(8,128)(2,1)}), bf16[16,6,64,256]{3,2,1,0:T(8,128)(2,1)}, u32[]{:S(2)}, u32[]{:S(2)}) %all-to-all-start.1) | async-done | bytes 3145760 | tf_op jit(solution)/shard_map/all_to_all | solution.py:218
  89.0 92.3 %attention.1 = (bf16[16,6,64,256]{3,2,1,0:T(8,128)(2,1)}, f32[16,6,256]{2,1,0:T(8,128)}) custom-call(s32[96]{0:T(128)} %reshape.115.ids, bf16[16,6,64,256]{3,2,1,0:T(8,128)(2,1)} %all-to-all-done.1.q_ref, bf16[24,128,256]{2,1,0:T(8,128)(2,1)} %get-tuple-element.17.k_ref, bf16[24,256,128]{2,1,0:T(8,128)(2,1)} %get-tuple-element.18.vt_ref), custom_call_target="tpu_custom_call" | custom-call | tf_op jit(solution)/shard_map/attention/pallas_call | solution.py:269
  181.2 1.6 reshape.126.lev_ref
  182.9 5.1 %merge.1 = bf16[768,256]{1,0:T(8,128)(2,1)} custom-call(s32[48]{0:T(128)} %copy-done.3, bf16[96,64,256]{2,1,0:T(8,128)(2,1)} %bitcast.28, f32[96,1,256]{2,1,0:T(1,128)} %reshape.126.lev_ref, f32[768,256]{1,0:T(8,128)} %fusion.6.gated_ref, f32[768,256]{1,0:T(8,128)} %fusion.3.blend_ref), custom_call_target="tpu_custom_call" | custom-call | tf_op jit(solution)/shard_map/merge/pallas_call | solution.py:285
  188.0 1.2 copy.57
  189.2 4.0 %all_to_all.33 = bf16[2,384,256]{1,2,0:T(8,128)(2,1)S(1)} all-to-all(bf16[2,384,256]{1,2,0:T(8,128)(2,1)S(1)} %copy.57), channel_id=1, replica_groups=mesh['st'=16,'tp'=2] {'tp'}, dimensions={0} | all-to-all | bytes 786432 | tf_op jit(solution)/shard_map/all_to_all | solution.py:307
  193.3 0.0 copy-done
  193.3 2.2 %convolution_convert_fusion = bf16[384,2048]{1,0:T(8,128)(2,1)} fusion(bf16[384,512]{0,1:T(8,128)(2,1)S(1)} %bitcast.30, bf16[512,2048]{1,0:T(8,128)(2,1)S(1)} %copy-done), kind=kOutput, calls=%fused_computation | convolution fusion | flops 806092800 | bytes 4063232 | tf_op jit(solution)/shard_map/dot_general | solution.py:308
  (3 shorter events, 0.0 us)
Async XLA Ops:
  0.0 193.3 %copy-start = (bf16[512,2048]{1,0:T(8,128)(2,1)S(1)}, bf16[512,2048]{1,0:T(8,128)(2,1)}, u32[]{:S(2)}) copy-start(bf16[512,2048]{1,0:T(8,128)(2,1)} %param.29) | copy-start | bytes 6291460
  2.3 19.0 %copy-start.3 = (s32[48]{0:T(128)}, s32[48]{0:T(128)S(1)}, u32[]{:S(2)}) copy-start(s32[48]{0:T(128)S(1)} %multiply_add_fusion.pos) | copy-start | bytes 580
  3.7 17.6 %all-to-all-start = ((s32[16,1,6]{2,1,0:T(1,128)}), s32[16,1,6]{2,1,0:T(1,128)S(1)}, u32[]{:S(2)}, u32[]{:S(2)}) async-start(s32[16,1,6]{2,1,0:T(1,128)} %bitcast), calls=%async_computation | async-start | bytes 16384 | tf_op jit(solution)/shard_map/all_to_all | solution.py:188
  21.3 67.7 %all-to-all-start.1 = ((bf16[16,6,64,256]{3,2,1,0:T(8,128)(2,1)}), bf16[16,6,64,256]{3,2,1,0:T(8,128)(2,1)}, u32[]{:S(2)}, u32[]{:S(2)}) async-start(bf16[16,6,64,256]{3,2,1,0:T(8,128)(2,1)} %bitcast.27), calls=%async_computation.1 | async-start | bytes 6291456 | tf_op jit(solution)/shard_map/all_to_all | solution.py:218
  28.2 7.4 %copy-start.4 = (f32[256]{0:T(256)S(1)}, f32[256]{0:T(256)}, u32[]{:S(2)}) copy-start(f32[256]{0:T(256)} %param.22) | copy-start | bytes 3076
  28.3 8.0 %copy-start.1 = (bf16[4,128,128]{2,1,0:T(8,128)(2,1)S(1)}, bf16[4,128,128]{2,1,0:T(8,128)(2,1)}, u32[]{:S(2)}) copy-start(bf16[4,128,128]{2,1,0:T(8,128)(2,1)} %param.23) | copy-start | bytes 393220
  28.3 8.0 %copy-start.2 = (f32[4,128]{1,0:T(4,128)S(1)}, f32[4,128]{1,0:T(4,128)}, u32[]{:S(2)}) copy-start(f32[4,128]{1,0:T(4,128)} %param.24) | copy-start | bytes 6148
where the time goes:
time: 196 us; the launch traced here: 195 us
  Pallas kernels  122 us (62%)
  waiting for transfers between devices  19.6 us (10%)
  matrix products  17.9 us (9%)
  starting transfers between devices  15.3 us (8%)
  local copies, waits for them, and re-layouts  10.2 us (5%)
  blocking collectives  6.55 us (3%)
  other arithmetic  3.29 us (2%)
    pallas_call x1, Pallas kernels, per_device(): pl.pallas_call(functools.partial(attention_kernel, local_heads, owner_cou...  92.3 us
    all_to_all x1, waiting for transfers between devices, per_device(): lax.all_to_all(sent.reshape(owner_count, cap, span_length, width), 'st',...  19.6 us
    pallas_call x1, Pallas kernels, per_device(): pl.pallas_call(store_kernel, grid=(store_count // group,), in_specs=[pl.B...  15.8 us
    pallas_call x1, Pallas kernels, per_device(): pl.pallas_call(functools.partial(query_kernel, span_length, slots), grid_...  9.21 us
    all_to_all x1, starting transfers between devices, per_device(): lax.all_to_all(slot_local.reshape(owner_count, cap), 'st', split_axis=0,...  8.34 us
    all_to_all x1, starting transfers between devices, per_device(): lax.all_to_all(sent.reshape(owner_count, cap, span_length, width), 'st',...  6.96 us
    dot_general x1, matrix products, per_device(): carry_branch = jnp.dot(normed, carry_weight, preferred_element_type=f32)  5.56 us
    pallas_call x1, Pallas kernels, per_device(): pl.pallas_call(functools.partial(merge_kernel, local_heads, spans, pick_c...  5.14 us
  transfers between devices with their start and end apart: 2, of which 1 were waited for; matrix products, arithmetic and copies ran while one was open for 12% of the time, Pallas kernels for 13%

commit v1 on v0

v1 whole, which is shorter than its diff:
```python
import functools

import jax
import jax.numpy as jnp
from jax import lax
from jax.experimental import pallas as pl
from jax.experimental.pallas import tpu as pltpu
from jax.sharding import PartitionSpec as P

norm_eps = 1e-06
bf16 = jnp.bfloat16
f32 = jnp.float32


def normed_rows(matrix, gain):
    values = matrix.astype(f32)
    scaled = values * lax.rsqrt(jnp.mean(values * values, axis=-1, keepdims=True) + norm_eps)
    return (scaled * gain).astype(bf16)

far = -1e30
MESH = pl.DeviceIdType.MESH


def query_kernel(span_length, tok_ref, gain_ref, wq_ref, normed_ref, q_ref):
    normed = normed_rows(tok_ref[...], gain_ref[...])
    normed_ref[...] = normed
    q = jnp.dot(normed, wq_ref[...], preferred_element_type=f32).astype(bf16)
    q_ref[...] = q.reshape(q_ref.shape)


def store_kernel(st_ref, gain_ref, wk_ref, wv_ref, k_ref, vt_ref):
    count, length, _ = st_ref.shape
    for p in range(count):
        normed = normed_rows(st_ref[p], gain_ref[...])
        k_ref[p] = jnp.dot(normed, wk_ref[...], preferred_element_type=f32).astype(bf16)
        v = jnp.dot(normed, wv_ref[...], preferred_element_type=f32)
        vt_ref[p] = v.T.astype(bf16)


def stacked_queries(q, heads):
    length, width = q.shape
    dim = width // heads
    row_head = lax.broadcasted_iota(jnp.int32, (heads * length, width), 0) // length
    lane_head = lax.broadcasted_iota(jnp.int32, (heads * length, width), 1) // dim
    return jnp.where(row_head == lane_head, jnp.concatenate([q] * heads, axis=0), jnp.zeros((), bf16))


def own_head(o, heads):
    width, columns = o.shape
    dim, length = width // heads, columns // heads
    col_head = lax.broadcasted_iota(jnp.int32, (dim, columns), 1) // length
    out = o[0:dim]
    for h in range(1, heads):
        out = jnp.where(col_head == h, o[h * dim : (h + 1) * dim], out)
    return out


def route_kernel(
    sizes,
    own_tab,
    tab_ref,
    q_ref,
    k_ref,
    vt_ref,
    gated_ref,
    blend_ref,
    out_ref,
    tabs_v,
    tabs_s,
    qcol,
    qout,
    qin,
    rout,
    lout,
    rin,
    lin,
    mout,
    mlout,
    mid,
    mlin,
    half,
    s_scr,
    w_scr,
    tab_send,
    tab_recv,
    loc,
    ring_send,
    ring_recv,
    qs,
    qr,
    rs,
    rr,
    ls,
    lr,
    ms,
    mr,
    mls,
    mlr,
    ts,
    tr,
):
    columns, plane, parts, heads, cap, picks = sizes
    n = columns * plane
    spans, length, width = q_ref.shape
    dim = width // heads
    scale = dim ** (-0.5)
    slots = n * cap
    local = plane * cap
    me = lax.axis_index("st")
    side = lax.axis_index("tp")
    z = me // plane
    p = me % plane
    base = z * local

    def remote(src, dst, send, recv, where):
        return pltpu.make_async_remote_copy(
            src_ref=src, dst_ref=dst, send_sem=send, recv_sem=recv, device_id=where, device_id_type=MESH
        )

    barrier = pltpu.get_barrier_semaphore()

    def greet(d, carry):
        pl.semaphore_signal(barrier, inc=1, device_id={"st": lax.rem(me + d, n)}, device_id_type=MESH)
        return carry

    lax.fori_loop(1, n, greet, 0)
    for d in range(1, parts):
        pl.semaphore_signal(barrier, inc=1, device_id={"tp": lax.rem(side + d, parts)}, device_id_type=MESH)
    pl.semaphore_wait(barrier, n - 1 + parts - 1)

    def mate(j):
        return {"st": z * plane + lax.rem(p + j, plane)}

    def back_mate(j):
        return {"st": z * plane + lax.rem(p + plane - j, plane)}

    def tab_copy(d):
        return remote(tab_ref, tabs_v.at[me], tab_send.at[d], tab_recv.at[d], {"st": lax.rem(me + d, n)})

    def ring_copy(s):
        src = q_ref if s == 0 else qcol[s - 1]
        where = {"st": lax.rem(z + 1, columns) * plane + p}
        return remote(src, qcol[s], ring_send.at[s], ring_recv.at[s], where)

    def query_copy(s, j):
        return remote(qout.at[s, j], qin.at[s, j], qs.at[s, j], qr.at[s, j], mate(j))

    def result_copies(s, j):
        mine = pl.ds(p * cap, cap)
        return (
            remote(rout.at[s, j], rin[s].at[mine], rs.at[s, j], rr.at[s, j], back_mate(j)),
            remote(lout.at[s, j], lin[s].at[mine], ls.at[s, j], lr.at[s, j], back_mate(j)),
        )

    def merged_copies(s):
        where = {"st": lax.rem(z + columns - s, columns) * plane + p}
        return (
            remote(mout.at[s - 1], mid.at[s - 1], ms.at[s - 1], mr.at[s - 1], where),
            remote(mlout.at[s - 1], mlin.at[s - 1], mls.at[s - 1], mlr.at[s - 1], where),
        )

    def look(s, j, i):
        row = lax.rem(z + columns - s, columns) * plane + lax.rem(p + plane - j, plane)
        return tabs_s[row, 0, i]

    def each(count, f, first=1):
        def body(i, carry):
            f(i)
            return carry

        lax.fori_loop(first, count, body, 0)

    each(n, lambda d: tab_copy(d).start())
    if columns > 1:
        ring_copy(0).start()
    own_copy = pltpu.make_async_copy(tab_ref, tabs_v.at[me], loc.at[0])
    own_copy.start()

    def select(s):
        block = q_ref if s == 0 else qcol[s - 1]

        def pick(j):
            o = z * plane + lax.rem(p + j, plane)
            for c in range(cap):
                i = slots + o * cap + c
                span = own_tab[i] if s == 0 else look(s, 0, i)
                qout[s, j, c] = block[span]

        each(plane, pick)
        each(plane, lambda j: query_copy(s, j).start())

    select(0)
    own_copy.wait()
    each(n, lambda d: tab_copy(d).wait_recv())
    to_smem = pltpu.make_async_copy(tabs_v, tabs_s, loc.at[1])
    to_smem.start()
    to_smem.wait()

    def attend(queries, passages, put):
        for c in range(cap):
            s_scr[c] = (
                lax.dot_general(
                    k_ref[passages[c]],
                    stacked_queries(queries[c], heads),
                    (((1,), (1,)), ((), ())),
                    preferred_element_type=f32,
                )
                * scale
            )
        totals = []
        levels = []
        for c in range(cap):
            s = s_scr[c]
            peak = jnp.max(s, axis=0, keepdims=True)
            w = jnp.exp(s - peak)
            total = jnp.sum(w, axis=0, keepdims=True)
            w_scr[c] = w.astype(bf16)
            totals.append(total)
            levels.append(peak + jnp.log(total))
        for c in range(cap):
            o = jnp.dot(vt_ref[passages[c]], w_scr[c], preferred_element_type=f32)
            put(c, (own_head(o, heads) / totals[c]).astype(bf16), levels[c])

    def attention(s):
        block = q_ref if s == 0 else qcol[s - 1]
        mine = me * cap
        spans_here = [look(s, 0, slots + mine + c) for c in range(cap)]
        passages = [look(s, 0, mine + c) for c in range(cap)]

        def put_here(c, value, level):
            rin[s][p * cap + c] = value
            lin[s][p * cap + c] = level

        attend([block[i] for i in spans_here], passages, put_here)

        def for_mate(j):
            query_copy(s, j).wait_recv()

            def put(c, value, level):
                rout[s, j, c] = value
                lout[s, j, c] = level

            attend([qin[s, j, c] for c in range(cap)], [look(s, j, mine + c) for c in range(cap)], put)

            @pl.when(j > 1)
            def _():
                for copy in result_copies(s, j - 1):
                    copy.start()

        each(plane, for_mate)
        if plane > 1:
            for copy in result_copies(s, plane - 1):
                copy.start()

    def gathered(s, span):
        levels, values = [], []
        for k in range(picks):
            i = look(s, 0, 2 * slots + span * picks + k) - base
            inside = (i >= 0) & (i < local)
            i = jnp.clip(i, 0, local - 1)
            levels.append(jnp.where(inside, lin[s][i], far))
            values.append(rin[s][i])
        return levels, values

    def weighted(levels, values):
        top = functools.reduce(jnp.maximum, levels)
        ws = [jnp.exp(level - top) for level in levels]
        total = sum(ws)
        summed = sum(w * value.astype(f32) for w, value in zip(ws, values))
        return summed / total, top + jnp.log(total)

    def wait_results(s):
        def one(j):
            for copy in result_copies(s, j):
                copy.wait_recv()

        each(plane, one)

    def merge(s):
        wait_results(s)

        def one(span):
            value, level = weighted(*gathered(s, span))
            mout[s - 1, span] = value.astype(bf16)
            mlout[s - 1, span] = level

        each(spans, one, 0)
        for copy in merged_copies(s):
            copy.start()

    for s in range(1, columns):
        ring_copy(s - 1).wait_recv()
        if s < columns - 1:
            ring_copy(s).start()
        select(s)
        if s > 1:
            attention(s - 1)
    if columns > 1:
        attention(columns - 1)
    for s in range(1, columns - 1):
        merge(s)
    attention(0)
    if columns > 1:
        merge(columns - 1)
    wait_results(0)
    for s in range(1, columns):
        for copy in merged_copies(s):
            copy.wait_recv()

    share = spans // parts
    rows = share * length

    def final(first, to):
        def one(i):
            span = first + i
            levels, values = gathered(0, span)
            for s in range(1, columns):
                levels.append(mlin[s - 1, span])
                values.append(mid[s - 1, span])
            memory, _ = weighted(levels, values)
            memory = memory.T
            memory = jnp.concatenate([memory[h * length : (h + 1) * length] for h in range(heads)], axis=1)
            at = pl.ds(pl.multiple_of(span * length, length), length)
            to(i, (gated_ref[at] + blend_ref[at] * memory).astype(bf16))

        each(share, one, 0)

    lanes = pl.ds(pl.multiple_of(side * width, width), width)

    def half_copy(d):
        return remote(half.at[d - 1], out_ref.at[:, lanes], ts.at[d - 1], tr.at[d - 1], {"tp": lax.rem(side + d, parts)})

    for d in range(1, parts):

        def keep(i, value):
            half[d - 1, pl.ds(pl.multiple_of(i * length, length), length)] = value

        final(lax.rem(side + d, parts) * share, keep)
        half_copy(d).start()

    def keep_own(i, value):
        out_ref[pl.ds(pl.multiple_of(i * length, length), length), lanes] = value

    final(side * share, keep_own)

    for d in range(1, parts):
        half_copy(d).wait()
    each(n, lambda d: tab_copy(d).wait_send())
    for s in range(columns - 1):
        ring_copy(s).wait_send()
    for s in range(columns):

        def done(j):
            query_copy(s, j).wait_send()
            for copy in result_copies(s, j):
                copy.wait_send()

        each(plane, done)
    for s in range(1, columns):
        for copy in merged_copies(s):
            copy.wait_send()


def per_device(
    tokens,
    route_ids,
    store,
    token_gain,
    store_gain,
    carry_weight,
    spatial_weight,
    spatial_gain,
    position_mix,
    position_bias,
    query_weight,
    key_weight,
    read_weight,
    blend_weight,
    output_weight,
):
    row_count, model = tokens.shape
    local_heads, block_length = position_mix.shape[:2]
    width = carry_weight.shape[1]
    head_dim = width // local_heads
    span_count, pick_count = route_ids.shape
    span_length = row_count // span_count
    store_count, passage_length = store.shape[:2]
    owner_count = lax.axis_size("st")
    requests = span_count * pick_count
    cap = max(1, 2 * requests // owner_count)
    slots = owner_count * cap

    flat_ids = route_ids.reshape(requests)
    owner = flat_ids // store_count
    order = jnp.arange(requests, dtype=jnp.int32)
    earlier = (owner[:, None] == owner[None, :]) & (order[None, :] < order[:, None])
    position = owner * cap + jnp.sum(earlier.astype(jnp.int32), axis=1)
    hit = position[None, :] == jnp.arange(slots, dtype=jnp.int32)[:, None]
    slot_local = jnp.sum(jnp.where(hit, (flat_ids % store_count)[None, :], 0), axis=1)
    slot_span = jnp.sum(jnp.where(hit, (order // pick_count)[None, :], 0), axis=1)
    table = jnp.concatenate([slot_local, slot_span, position])
    table = jnp.pad(table, (0, -table.shape[0] % 128))

    tile = 2 * span_length
    normed, queries = pl.pallas_call(
        functools.partial(query_kernel, span_length),
        grid=(row_count // tile,),
        in_specs=[
            pl.BlockSpec((tile, model), lambda i: (i, 0)),
            pl.BlockSpec((1, model), lambda i: (0, 0)),
            pl.BlockSpec((model, width), lambda i: (0, 0)),
        ],
        out_specs=[
            pl.BlockSpec((tile, model), lambda i: (i, 0)),
            pl.BlockSpec((tile // span_length, span_length, width), lambda i: (i, 0, 0)),
        ],
        out_shape=[
            jax.ShapeDtypeStruct((row_count, model), bf16),
            jax.ShapeDtypeStruct((span_count, span_length, width), bf16),
        ],
        cost_estimate=pl.CostEstimate(
            flops=2 * row_count * model * width, bytes_accessed=4 * row_count * model, transcendentals=0
        ),
        name="query",
    )(tokens, token_gain.reshape(1, model), query_weight)

    group = 2
    keys, values_t = pl.pallas_call(
        store_kernel,
        grid=(store_count // group,),
        in_specs=[
            pl.BlockSpec((group, passage_length, model), lambda i: (i, 0, 0)),
            pl.BlockSpec((1, model), lambda i: (0, 0)),
            pl.BlockSpec((model, width), lambda i: (0, 0)),
            pl.BlockSpec((model, width), lambda i: (0, 0)),
        ],
        out_specs=[
            pl.BlockSpec((group, passage_length, width), lambda i: (i, 0, 0)),
            pl.BlockSpec((group, width, passage_length), lambda i: (i, 0, 0)),
        ],
        out_shape=[
            jax.ShapeDtypeStruct((store_count, passage_length, width), bf16),
            jax.ShapeDtypeStruct((store_count, width, passage_length), bf16),
        ],
        cost_estimate=pl.CostEstimate(
            flops=4 * store_count * passage_length * model * width,
            bytes_accessed=2 * store_count * passage_length * model,
            transcendentals=0,
        ),
        name="store",
    )(store, store_gain.reshape(1, model), key_weight, read_weight)

    carry_branch = jnp.dot(normed, carry_weight, preferred_element_type=f32)
    spatial = jax.nn.gelu(jnp.dot(normed, spatial_weight, preferred_element_type=f32), approximate=False)
    total_width = width * lax.axis_size("tp")
    moment_one, moment_two = lax.psum(
        (jnp.sum(spatial, axis=1), jnp.sum(spatial * spatial, axis=1)), "tp"
    )
    channel_mean = (moment_one / total_width)[:, None]
    channel_spread = (moment_two / total_width)[:, None] - channel_mean * channel_mean
    spatial_in = (
        (spatial - channel_mean) * lax.rsqrt(channel_spread + norm_eps) * spatial_gain
    ).astype(bf16)
    blocks = spatial_in.reshape(row_count // block_length, block_length, local_heads, head_dim)
    mixed_blocks = jnp.einsum("hij,njhc->nihc", position_mix, blocks, preferred_element_type=f32)
    mixed_blocks = mixed_blocks + position_bias.T[None, :, :, None]
    gated_mix = jax.nn.gelu(carry_branch, approximate=False) * mixed_blocks.reshape(row_count, width)
    blend_gate = jax.nn.sigmoid(jnp.dot(normed, blend_weight, preferred_element_type=f32))

    parts = lax.axis_size("tp")
    columns = 4 if owner_count % 4 == 0 else 1
    plane = owner_count // columns
    local = plane * cap
    wide = local_heads * span_length
    vmem = pl.BlockSpec(memory_space=pltpu.VMEM)
    smem = pl.BlockSpec(memory_space=pltpu.SMEM)
    dma = pltpu.SemaphoreType.DMA
    by_rows = pl.pallas_call(
        functools.partial(route_kernel, (columns, plane, parts, local_heads, cap, pick_count)),
        in_specs=[smem] + [vmem] * 6,
        out_specs=vmem,
        out_shape=jax.ShapeDtypeStruct((row_count // parts, parts * width), bf16),
        scratch_shapes=[
            pltpu.VMEM((owner_count, 1, table.shape[0]), jnp.int32),
            pltpu.SMEM((owner_count, 1, table.shape[0]), jnp.int32),
            [pltpu.VMEM((span_count, span_length, width), bf16)] * columns,
            pltpu.VMEM((columns, plane, cap, span_length, width), bf16),
            pltpu.VMEM((columns, plane, cap, span_length, width), bf16),
            pltpu.VMEM((columns, plane, cap, head_dim, wide), bf16),
            pltpu.VMEM((columns, plane, cap, 1, wide), f32),
            [pltpu.VMEM((local, head_dim, wide), bf16)] * columns,
            [pltpu.VMEM((local, 1, wide), f32)] * columns,
            pltpu.VMEM((columns, span_count, head_dim, wide), bf16),
            pltpu.VMEM((columns, span_count, 1, wide), f32),
            pltpu.VMEM((columns, span_count, head_dim, wide), bf16),
            pltpu.VMEM((columns, span_count, 1, wide), f32),
            pltpu.VMEM((parts, row_count // parts, width), bf16),
            pltpu.VMEM((cap, passage_length, wide), f32),
            pltpu.VMEM((cap, passage_length, wide), bf16),
            dma((owner_count,)),
            dma((owner_count,)),
            dma((2,)),
            dma((columns,)),
            dma((columns,)),
            dma((columns, plane)),
            dma((columns, plane)),
            dma((columns, plane)),
            dma((columns, plane)),
            dma((columns, plane)),
            dma((columns, plane)),
            dma((columns,)),
            dma((columns,)),
            dma((columns,)),
            dma((columns,)),
            dma((parts,)),
            dma((parts,)),
        ],
        compiler_params=pltpu.CompilerParams(
            collective_id=0, has_side_effects=True, vmem_limit_bytes=48 * 2**20
        ),
        name="route",
    )(table, table.reshape(1, table.shape[0]), queries, keys, values_t, gated_mix, blend_gate)
    return jnp.dot(by_rows, output_weight, preferred_element_type=f32).astype(bf16)


def solution(mesh):
    in_specs = (
        P("st", None),
        P("st", None),
        P("st", None, None),
        P(),
        P(),
        P(None, "tp"),
        P(None, "tp"),
        P("tp"),
        P("tp", None, None),
        P("tp", None),
        P(None, "tp"),
        P(None, "tp"),
        P(None, "tp"),
        P(None, "tp"),
        P(),
    )
    out_specs = P(("st", "tp"), None)
    return jax.shard_map(
        per_device, mesh=mesh, in_specs=in_specs, out_specs=out_specs, check_vma=False
    )
```

time: 196 us -> 150 us (0.77)
  waiting for transfers between devices: 19.6 us -> 0 us
  starting transfers between devices: 15.3 us -> 0 us
  Pallas kernels: 122 us -> 117 us
  blocking collectives: 6.55 us -> 2.66 us
  other arithmetic: 3.29 us -> 0.68 us
    all_to_all x2 -> x0, waiting for transfers between devices: 19.6 us -> none  [the longest x1 19.6 us: per_device(): lax.all_to_all(sent.reshape(owner_count, cap, span_length, width), 'st',...]
    all_to_all x2 -> x0, starting transfers between devices: 15.3 us -> none  [the longest x1 8.34 us: per_device(): lax.all_to_all(slot_local.reshape(owner_count, cap), 'st', split_axis=0,...]
    pallas_call x3 -> x2, Pallas kernels: 107 us -> 102 us  [the longest x1 95.2 us: per_device(): pl.pallas_call(functools.partial(route_kernel, (columns, plane, parts, lo...]
    all_to_all x1 -> x0, blocking collectives: 4.05 us -> none  [per_device(): lax.all_to_all(mixed_rows, 'tp', split_axis=0, concat_axis=1, tiled=True)]
    unnamed x10 -> x18, local copies, waits for them, and re-layouts: 0.03 us -> 3.97 us
    all_to_all x3 -> x0, local copies, waits for them, and re-layouts: 2.41 us -> none  [the longest x1 1.21 us: per_device(): lax.all_to_all(mixed_rows, 'tp', split_axis=0, concat_axis=1, tiled=True)]
    reshape x2 -> x0, local copies, waits for them, and re-layouts: 2.2 us -> none  [the longest x1 1.63 us: per_device(): back_levels.reshape(slots, 1, local_heads * span_length)]
  transfers between devices with their start and end apart: 2 -> 0, of which waited for: 1 -> 0; matrix products, arithmetic and copies ran while one was open for 12% -> 0% of each run, Pallas kernels for 13% -> 0%
where the time goes in v1:
time: 150 us; the launch traced here: 148 us
  Pallas kernels  117 us (78%)
  matrix products  17.2 us (11%)
  local copies, waits for them, and re-layouts  10.3 us (7%)
  blocking collectives  2.66 us (2%)
    pallas_call x1, Pallas kernels, per_device(): pl.pallas_call(functools.partial(route_kernel, (columns, plane, parts, lo...  95.2 us
    pallas_call x1, Pallas kernels, per_device(): pl.pallas_call(store_kernel, grid=(store_count // group,), in_specs=[pl.B...  15.8 us
    pallas_call x1, Pallas kernels, per_device(): pl.pallas_call(functools.partial(query_kernel, span_length), grid=(row_co...  6.34 us
    reshape x2, local copies, waits for them, and re-layouts, per_device(): mixed_blocks.reshape(row_count, width)  5.41 us
    dot_general x1, matrix products, per_device(): carry_branch = jnp.dot(normed, carry_weight, preferred_element_type=f32)  4.91 us
    dot_general x1, matrix products, per_device(): jnp.dot(normed, spatial_weight, preferred_element_type=f32)  4.86 us
    dot_general x1, matrix products, per_device(): jnp.dot(normed, blend_weight, preferred_element_type=f32)  4.06 us
    unnamed x18, local copies, waits for them, and re-layouts  3.97 us

profile of v1, /device:TPU:0, one launch (start us, length us, event | category | flops | bytes accessed | tf_op | source)
XLA Modules:
  0.0 148.3 jit_solution(12878678625599091148)
XLA Ops:
  0.0 0.0 copy-start
  0.0 6.3 %query.1 = (bf16[768,2048]{1,0:T(8,128)(2,1)}, bf16[12,64,256]{2,1,0:T(8,128)(2,1)}) custom-call(bf16[768,2048]{1,0:T(8,128)(2,1)} %tok_ref.1, f32[1,2048]{1,0:T(1,128)} %bitcast.22, bf16[2048,256]{1,0:T(8,128)(2,1)} %wq_ref.1), custom_call_target="tpu_custom_call" | custom-call | flops 805306368 | bytes 6291456 | tf_op jit(solution)/shard_map/query/pallas_call | solution.py:405
  6.3 0.0 copy-start.8
  6.3 0.0 copy-start.5
  6.3 0.0 copy-start.7
  6.4 4.9 %fusion.26 = (f32[768]{0:T(1024)S(1)}, f32[768]{0:T(1024)S(1)}, f32[768,256]{1,0:T(8,128)S(1)}) fusion(bf16[768,2048]{1,0:T(8,128)(2,1)} %get-tuple-element.12, bf16[2048,256]{1,0:T(8,128)(2,1)} %param.21), kind=kOutput, calls=%fused_computation.67 | convolution fusion | flops 818477568 | bytes 4986880 | tf_op jit(solution)/shard_map/dot_general | solution.py:454
  11.2 2.7 %all-reduce.1 = (f32[768]{0:T(1024)S(1)}, f32[768]{0:T(1024)S(1)}) all-reduce(f32[768]{0:T(1024)S(1)} %get-tuple-element.14, f32[768]{0:T(1024)S(1)} %get-tuple-element.13), channel_id=1, replica_groups=mesh['st'=16,'tp'=2] {'tp'}, use_global_device_ids=true, to_apply=%region_6.7 | all-reduce | flops 1536 | bytes 12288 | tf_op jit(solution)/shard_map/psum | solution.py:456
  13.9 0.0 copy-done.8
  13.9 0.3 multiply_convert_fusion
  14.2 0.3 reshape.104
  14.5 0.0 copy-done.5
  14.5 0.0 copy-done.7
  14.5 1.3 fusion.1
  15.8 2.4 %copy.45 = f32[6,128,4,64]{3,2,1,0:T(4,128)} copy(f32[6,128,4,64]{1,3,0,2:T(8,128)} %fusion.1) | data formatting | bytes 1572864 | tf_op jit(solution)/shard_map/reshape | solution.py:467
  18.2 3.0 %reshape.105 = f32[768,256]{1,0:T(8,128)} reshape(f32[6,128,4,64]{3,2,1,0:T(4,128)} %copy.45) | data formatting | bytes 1572864 | tf_op jit(solution)/shard_map/reshape | solution.py:467
  21.2 0.0 copy-start.6
  21.2 4.9 %fusion.6.gated_ref = f32[768,256]{1,0:T(8,128)S(1)} fusion(f32[768,256]{1,0:T(8,128)} %reshape.105, bf16[768,2048]{1,0:T(8,128)(2,1)} %get-tuple-element.12, bf16[2048,256]{1,0:T(8,128)(2,1)} %param.20), kind=kOutput, calls=%fused_computation.11 | convolution fusion | flops 818085888 | bytes 5767168 | tf_op jit(solution)/shard_map/dot_general | solution.py:453
  26.1 0.0 copy-done.6
  26.1 0.1 copy.34
  26.2 0.1 div.36
  26.3 0.1 copy.33
  26.4 0.1 rem.39
  26.5 0.1 copy.32
  26.6 0.1 ne.74
  26.7 0.2 convert_reduce_fusion
  26.9 0.1 select_reduce_fusion.1
  27.0 0.1 pad_add_fusion
  27.1 4.1 %fusion.3.blend_ref = f32[768,256]{1,0:T(8,128)} fusion(bf16[768,2048]{1,0:T(8,128)(2,1)} %get-tuple-element.12, bf16[2048,256]{1,0:T(8,128)(2,1)} %param.28), kind=kOutput, calls=%fused_computation.6 | convolution fusion | flops 805896192 | bytes 4980736 | tf_op jit(solution)/shard_map/dot_general | solution.py:468
  31.2 0.0 copy-start.4
  31.2 15.8 %store.1 = (bf16[24,128,256]{2,1,0:T(8,128)(2,1)}, bf16[24,256,128]{2,1,0:T(8,128)(2,1)}) custom-call(bf16[24,128,2048]{2,1,0:T(8,128)(2,1)} %st_ref.1, f32[1,2048]{1,0:T(1,128)} %bitcast.24, bf16[2048,256]{1,0:T(8,128)(2,1)} %wk_ref.1, bf16[2048,256]{1,0:T(8,128)(2,1)} %wv_ref.1), custom_call_target="tpu_custom_call" | custom-call | flops 6442450944 | bytes 12582912 | tf_op jit(solution)/shard_map/store/pallas_call | solution.py:428
  47.0 0.0 copy-done.4
  47.0 0.0 copy-start.1
  47.0 1.4 copy-done.1
  48.4 0.0 copy-start.2
  48.4 1.4 copy-done.2
  49.8 0.0 copy-start.3
  49.8 1.1 copy-done.3
  51.0 95.2 %route.1 = bf16[384,512]{1,0:T(8,128)(2,1)S(1)} custom-call(s32[256]{0:T(256)S(1)} %pad.4.own_tab, s32[1,256]{1,0:T(1,128)S(1)} %bitcast.21, bf16[12,64,256]{2,1,0:T(8,128)(2,1)S(1)} %copy-done.4, bf16[24,128,256]{2,1,0:T(8,128)(2,1)S(1)} %copy-done.1, bf16[24,256,128]{2,1,0:T(8,128)(2,1)S(1)} %copy-done.2, f32[768,256]{1,0:T(8,128)S(1)} %fusion.6.gated_ref, ...), custom_call_target="tpu_custom_call" | custom-call | tf_op jit(solution)/shard_map/route/pallas_call | solution.py:478
  146.2 0.0 copy-done
  146.2 2.1 %convolution_convert_fusion = bf16[384,2048]{1,0:T(8,128)(2,1)} fusion(bf16[384,512]{1,0:T(8,128)(2,1)S(1)} %route.1, bf16[512,2048]{1,0:T(8,128)(2,1)S(1)} %copy-done), kind=kOutput, calls=%fused_computation | convolution fusion | flops 806092800 | bytes 4063232 | tf_op jit(solution)/shard_map/dot_general | solution.py:523
  (6 shorter events, 0.0 us)
Async XLA Ops:
  0.0 146.2 %copy-start = (bf16[512,2048]{1,0:T(8,128)(2,1)S(1)}, bf16[512,2048]{1,0:T(8,128)(2,1)}, u32[]{:S(2)}) copy-start(bf16[512,2048]{1,0:T(8,128)(2,1)} %param.29) | copy-start | bytes 6291460
  6.3 7.5 %copy-start.8 = (f32[256]{0:T(256)S(1)}, f32[256]{0:T(256)}, u32[]{:S(2)}) copy-start(f32[256]{0:T(256)} %param.22) | copy-start | bytes 3076
  6.3 8.2 %copy-start.5 = (bf16[4,128,128]{2,1,0:T(8,128)(2,1)S(1)}, bf16[4,128,128]{2,1,0:T(8,128)(2,1)}, u32[]{:S(2)}) copy-start(bf16[4,128,128]{2,1,0:T(8,128)(2,1)} %param.23) | copy-start | bytes 393220
  6.3 8.2 %copy-start.7 = (f32[4,128]{1,0:T(4,128)S(1)}, f32[4,128]{1,0:T(4,128)}, u32[]{:S(2)}) copy-start(f32[4,128]{1,0:T(4,128)} %param.24) | copy-start | bytes 6148
  21.2 4.9 %copy-start.6 = (s32[12,4]{0,1:T(4,128)S(1)}, s32[12,4]{0,1:T(4,128)}, u32[]{:S(2)}) copy-start(s32[12,4]{0,1:T(4,128)} %param.16) | copy-start | bytes 580
  31.2 15.8 %copy-start.4 = (bf16[12,64,256]{2,1,0:T(8,128)(2,1)S(1)}, bf16[12,64,256]{2,1,0:T(8,128)(2,1)}, u32[]{:S(2)}) copy-start(bf16[12,64,256]{2,1,0:T(8,128)(2,1)} %get-tuple-element.9.q_ref) | copy-start | bytes 1179652
  47.0 1.4 copy-start.1
  48.4 1.4 copy-start.2
  49.8 1.1 copy-start.3

commit v2 on v1

v2 whole, which is shorter than its diff:
```python
import functools

import jax
import jax.numpy as jnp
from jax import lax
from jax.experimental import pallas as pl
from jax.experimental.pallas import tpu as pltpu
from jax.sharding import PartitionSpec as P

norm_eps = 1e-06
bf16 = jnp.bfloat16
f32 = jnp.float32


def normed_rows(matrix, gain):
    values = matrix.astype(f32)
    scaled = values * lax.rsqrt(jnp.mean(values * values, axis=-1, keepdims=True) + norm_eps)
    return (scaled * gain).astype(bf16)

far = -1e30
MESH = pl.DeviceIdType.MESH


def stacked_queries(q, heads):
    length, width = q.shape
    dim = width // heads
    row_head = lax.broadcasted_iota(jnp.int32, (heads * length, width), 0) // length
    lane_head = lax.broadcasted_iota(jnp.int32, (heads * length, width), 1) // dim
    return jnp.where(row_head == lane_head, jnp.concatenate([q] * heads, axis=0), jnp.zeros((), bf16))


def own_head(o, heads):
    width, columns = o.shape
    dim, length = width // heads, columns // heads
    col_head = lax.broadcasted_iota(jnp.int32, (dim, columns), 1) // length
    out = o[0:dim]
    for h in range(1, heads):
        out = jnp.where(col_head == h, o[h * dim : (h + 1) * dim], out)
    return out


def erf_gelu(x):
    return 0.5 * x * (1.0 + lax.erf(x * 0.5**0.5))


def layer_kernel(
    sizes,
    own_tab,
    tab_ref,
    token_gain,
    store_gain,
    spatial_gain,
    bias_ref,
    mix_ref,
    tokens,
    store,
    wq,
    ws,
    wk,
    wv,
    wc,
    wb,
    out_ref,
    v,
):
    columns, plane, parts, heads, cap, picks, halves = sizes
    q_own, qcol, qout, qin = v["q_own"], v["qcol"], v["qout"], v["qin"]
    rout, lout, rin, lin = v["rout"], v["lout"], v["rin"], v["lin"]
    mout, mlout, mid, mlin, half = v["mout"], v["mlout"], v["mid"], v["mlin"], v["half"]
    tabs_v, tabs_s, normed = v["tabs_v"], v["tabs_s"], v["normed"]
    keys, values_t, w_ref = v["keys"], v["values_t"], v["w"]
    n = columns * plane
    spans, length, width = q_own.shape
    tiles, tile, model = normed.shape
    per = tile // length
    store_count = keys.shape[0]
    dim = width // heads
    scale = dim ** (-0.5)
    slots = n * cap
    local = plane * cap
    me = lax.axis_index("st")
    side = lax.axis_index("tp")
    z = me // plane
    p = me % plane
    base = z * local

    def each(count, f, first=0):
        def body(i, carry):
            f(i)
            return carry

        lax.fori_loop(first, count, body, 0)

    def remote(src, dst, send, recv, where):
        return pltpu.make_async_remote_copy(
            src_ref=src, dst_ref=dst, send_sem=send, recv_sem=recv, device_id=where, device_id_type=MESH
        )

    def token_copy(i):
        rows = pl.ds(pl.multiple_of(i * tile, tile), tile)
        return pltpu.make_async_copy(tokens.at[rows], v["tok"].at[i], v["tok_sem"].at[i])

    def store_copy(i):
        return pltpu.make_async_copy(store.at[i], v["st"].at[i], v["st_sem"].at[i])

    def weight_copy(i):
        return pltpu.make_async_copy((wq, ws, wk, wv, wc, wb)[i], w_ref.at[i], v["w_sem"].at[i])

    def mate(j):
        return {"st": z * plane + lax.rem(p + j, plane)}

    def back_mate(j):
        return {"st": z * plane + lax.rem(p + plane - j, plane)}

    def other(d):
        return {"tp": lax.rem(side + d, parts)}

    def tab_copy(d):
        return remote(tab_ref, tabs_v.at[me], v["tab_send"].at[d], v["tab_recv"].at[d], {"st": lax.rem(me + d, n)})

    def block(s):
        return q_own if s == 0 else qcol[s - 1]

    def ring_copy(s, h):
        piece = pl.ds(h * (spans // halves), spans // halves)
        where = {"st": lax.rem(z + 1, columns) * plane + p}
        send, recv = v["ring_send"].at[s, h], v["ring_recv"].at[s, h]
        return remote(block(s).at[piece], qcol[s].at[piece], send, recv, where)

    def query_copy(s, j):
        return remote(qout.at[s, j], qin.at[s, j], v["qs"].at[s, j], v["qr"].at[s, j], mate(j))

    def result_copies(s, j):
        mine = pl.ds(p * cap, cap)
        return (
            remote(rout.at[s, j], rin[s].at[mine], v["rs"].at[s, j], v["rr"].at[s, j], back_mate(j)),
            remote(lout.at[s, j], lin[s].at[mine], v["ls"].at[s, j], v["lr"].at[s, j], back_mate(j)),
        )

    def merged_copies(s):
        where = {"st": lax.rem(z + columns - s, columns) * plane + p}
        i = s - 1
        return (
            remote(mout.at[i], mid.at[i], v["ms"].at[i], v["mr"].at[i], where),
            remote(mlout.at[i], mlin.at[i], v["mls"].at[i], v["mlr"].at[i], where),
        )

    def moment_copy(d):
        return remote(v["mom"], v["mom_in"].at[d - 1], v["xs"].at[d - 1], v["xr"].at[d - 1], other(d))

    def look(s, j, i):
        row = lax.rem(z + columns - s, columns) * plane + lax.rem(p + plane - j, plane)
        return tabs_s[row, 0, i]

    weight_copy(0).start()
    each(tiles, lambda i: token_copy(i).start())
    for i in range(1, 6):
        weight_copy(i).start()
    each(store_count, lambda i: store_copy(i).start())

    barrier = pltpu.get_barrier_semaphore()

    def greet(d):
        pl.semaphore_signal(barrier, inc=1, device_id={"st": lax.rem(me + d, n)}, device_id_type=MESH)

    each(n, greet, 1)
    for d in range(1, parts):
        pl.semaphore_signal(barrier, inc=1, device_id=other(d), device_id_type=MESH)

    weight_copy(0).wait()

    def query(i):
        token_copy(i).wait()
        rows = normed_rows(v["tok"][i], token_gain[...])
        normed[i] = rows
        q = jnp.dot(rows, w_ref[0], preferred_element_type=f32).astype(bf16)
        for s in range(per):
            q_own[i * per + s] = q[s * length : (s + 1) * length]

    for h in range(halves):
        each(tiles * (h + 1) // halves, query, tiles * h // halves)
        if h == 0:
            pl.semaphore_wait(barrier, n - 1 + parts - 1)
        if columns > 1:
            ring_copy(0, h).start()
    each(n, lambda d: tab_copy(d).start(), 1)
    own_copy = pltpu.make_async_copy(tab_ref, tabs_v.at[me], v["loc"].at[0])
    own_copy.start()

    def select(s):
        def pick(j):
            o = z * plane + lax.rem(p + j, plane)
            for c in range(cap):
                i = slots + o * cap + c
                span = own_tab[i] if s == 0 else look(s, 0, i)
                qout[s, j, c] = block(s)[span]

        each(plane, pick, 1)
        each(plane, lambda j: query_copy(s, j).start(), 1)

    select(0)

    def spatial_first(i):
        x = jnp.dot(normed[i], w_ref[1], preferred_element_type=f32)
        x = erf_gelu(x)
        v["spatial"][i] = x
        one = jnp.sum(x, axis=1, keepdims=True)
        two = jnp.sum(x * x, axis=1, keepdims=True)
        lane = lax.broadcasted_iota(jnp.int32, (tile, 128), 1)
        v["mom"][i] = jnp.where(lane < 64, one, two)

    weight_copy(1).wait()
    each(tiles, spatial_first)
    for d in range(1, parts):
        moment_copy(d).start()

    def project(i):
        store_copy(i).wait()
        rows = normed_rows(v["st"][i], store_gain[...])
        keys[i] = jnp.dot(rows, w_ref[2], preferred_element_type=f32).astype(bf16)
        values_t[i] = jnp.dot(rows, w_ref[3], preferred_element_type=f32).T.astype(bf16)

    def spatial_rest():
        for d in range(1, parts):
            moment_copy(d).wait_recv()
        weight_copy(4).wait()
        weight_copy(5).wait()

        def one(i):
            mom = v["mom"][i]
            for d in range(1, parts):
                mom = mom + v["mom_in"][d - 1, i]
            mom = mom / (width * parts)
            mean = mom[:, 0:1]
            spread = mom[:, 64:65] - mean * mean
            x = (v["spatial"][i] - mean) * lax.rsqrt(spread + norm_eps) * spatial_gain[...]
            x = x.astype(bf16)
            mixed = [
                jnp.dot(mix_ref[h], x[:, h * dim : (h + 1) * dim], preferred_element_type=f32)
                + bias_ref[:, h : h + 1]
                for h in range(heads)
            ]
            mixed = jnp.concatenate(mixed, axis=1)
            carry = jnp.dot(normed[i], w_ref[4], preferred_element_type=f32)
            v["gated"][i] = erf_gelu(carry) * mixed
            v["blend"][i] = jax.nn.sigmoid(jnp.dot(normed[i], w_ref[5], preferred_element_type=f32))

        each(tiles, one)

    def attend(queries, passages, put):
        for c in range(cap):
            v["s"][c] = (
                lax.dot_general(
                    keys[passages[c]],
                    stacked_queries(queries[c], heads),
                    (((1,), (1,)), ((), ())),
                    preferred_element_type=f32,
                )
                * scale
            )
        totals = []
        levels = []
        for c in range(cap):
            s = v["s"][c]
            peak = jnp.max(s, axis=0, keepdims=True)
            w = jnp.exp(s - peak)
            total = jnp.sum(w, axis=0, keepdims=True)
            v["p"][c] = w.astype(bf16)
            totals.append(total)
            levels.append(peak + jnp.log(total))
        for c in range(cap):
            o = jnp.dot(values_t[passages[c]], v["p"][c], preferred_element_type=f32)
            put(c, (own_head(o, heads) / totals[c]).astype(bf16), levels[c])

    def send_results(s, j):
        for copy in result_copies(s, j):
            copy.start()

    def attention(s, send=True):
        mine = me * cap

        def for_mate(j):
            query_copy(s, j).wait_recv()

            def put(c, value, level):
                rout[s, j, c] = value
                lout[s, j, c] = level

            attend([qin[s, j, c] for c in range(cap)], [look(s, j, mine + c) for c in range(cap)], put)
            if send:

                @pl.when(j > 1)
                def _():
                    send_results(s, j - 1)

        each(plane, for_mate, 1)

        def put_here(c, value, level):
            rin[s][p * cap + c] = value
            lin[s][p * cap + c] = level

        here = [block(s)[look(s, 0, slots + mine + c)] for c in range(cap)]
        if send and plane > 1:
            send_results(s, plane - 1)
        attend(here, [look(s, 0, mine + c) for c in range(cap)], put_here)

    def source(s, span, k):
        i = look(s, 0, 2 * slots + span * picks + k) - base
        return jnp.clip(i, 0, local - 1), (i >= 0) & (i < local)

    def weigh(s, more):
        def one(span):
            for k in range(picks):
                i, inside = source(s, span, k)
                v["lev"][k, pl.ds(span, 1)] = jnp.where(inside, lin[s][i], far)

        each(spans, one)
        levels = [v["lev"][k] for k in range(picks)] + more
        top = functools.reduce(jnp.maximum, levels)
        ws = [jnp.exp(level - top) for level in levels]
        total = sum(ws)
        for k, w in enumerate(ws):
            v["wt"][k] = w / total
        return top + jnp.log(total)

    def summed(s, span, more):
        at = pl.ds(span, 1)
        terms = [v["wt"][k, at] * rin[s][source(s, span, k)[0]].astype(f32) for k in range(picks)]
        for k, ref in enumerate(more):
            terms.append(v["wt"][picks + k, at] * ref[span].astype(f32))
        return sum(terms)

    def wait_results(s):
        def one(j):
            for copy in result_copies(s, j):
                copy.wait_recv()

        each(plane, one, 1)

    def merge(s):
        wait_results(s)
        mlout[s - 1] = weigh(s, [])

        def one(span):
            mout[s - 1, span] = summed(s, span, []).astype(bf16)

        each(spans, one)
        for copy in merged_copies(s):
            copy.start()

    own_copy.wait()
    weight_copy(2).wait()
    weight_copy(3).wait()
    steps = max(columns - 1, 1)
    cut = [store_count * min(i, 2) // 2 for i in range(steps + 1)] if steps > 1 else [0, store_count]
    for s in range(1, columns):
        each(cut[s], project, cut[s - 1])
        if s == 1:
            each(n, lambda d: tab_copy(d).wait_recv(), 1)
            to_smem = pltpu.make_async_copy(tabs_v, tabs_s, v["loc"].at[1])
            to_smem.start()
            to_smem.wait()
        for h in range(halves):
            ring_copy(s - 1, h).wait_recv()
            if s < columns - 1:
                ring_copy(s, h).start()
        select(s)
        if s > 1:
            attention(s - 1)
        if s == 2:
            spatial_rest()
    if columns > 1:
        attention(columns - 1)
    attention(0)
    for s in range(1, columns):
        merge(s)
    wait_results(0)
    for s in range(1, columns):
        for copy in merged_copies(s):
            copy.wait_recv()

    share = spans // parts
    weigh(0, [mlin[s - 1] for s in range(1, columns)])
    lanes = pl.ds(pl.multiple_of(side * width, width), width)

    def final(first, to):
        def one(i):
            span = first + i
            memory = summed(0, span, [mid.at[s - 1] for s in range(1, columns)]).T
            memory = jnp.concatenate([memory[h * length : (h + 1) * length] for h in range(heads)], axis=1)
            at = pl.ds(pl.multiple_of(lax.rem(span, per) * length, length), length)
            t = span // per
            to(i, (v["gated"][t, at] + v["blend"][t, at] * memory).astype(bf16))

        each(share, one)

    def half_copy(d):
        i = d - 1
        return remote(half.at[i], out_ref.at[:, lanes], v["ts"].at[i], v["tr"].at[i], other(d))

    def rows_of(i):
        return pl.ds(pl.multiple_of(i * length, length), length)

    for d in range(1, parts):

        def keep(i, value):
            half[d - 1, rows_of(i)] = value

        final(lax.rem(side + d, parts) * share, keep)
        half_copy(d).start()

    def keep_own(i, value):
        out_ref[rows_of(i), lanes] = value

    final(side * share, keep_own)

    for d in range(1, parts):
        half_copy(d).wait()
        moment_copy(d).wait_send()
    each(n, lambda d: tab_copy(d).wait_send(), 1)
    for s in range(columns - 1):
        for h in range(halves):
            ring_copy(s, h).wait_send()
    for s in range(columns):

        def done(j):
            query_copy(s, j).wait_send()
            for copy in result_copies(s, j):
                copy.wait_send()

        each(plane, done, 1)
    for s in range(1, columns):
        for copy in merged_copies(s):
            copy.wait_send()


def per_device(
    tokens,
    route_ids,
    store,
    token_gain,
    store_gain,
    carry_weight,
    spatial_weight,
    spatial_gain,
    position_mix,
    position_bias,
    query_weight,
    key_weight,
    read_weight,
    blend_weight,
    output_weight,
):
    row_count, model = tokens.shape
    local_heads, block_length = position_mix.shape[:2]
    width = carry_weight.shape[1]
    head_dim = width // local_heads
    span_count, pick_count = route_ids.shape
    span_length = row_count // span_count
    store_count, passage_length = store.shape[:2]
    owner_count = lax.axis_size("st")
    requests = span_count * pick_count
    cap = max(1, 2 * requests // owner_count)
    slots = owner_count * cap

    flat_ids = route_ids.reshape(requests)
    owner = flat_ids // store_count
    order = jnp.arange(requests, dtype=jnp.int32)
    earlier = (owner[:, None] == owner[None, :]) & (order[None, :] < order[:, None])
    position = owner * cap + jnp.sum(earlier.astype(jnp.int32), axis=1)
    hit = position[None, :] == jnp.arange(slots, dtype=jnp.int32)[:, None]
    slot_local = jnp.sum(jnp.where(hit, (flat_ids % store_count)[None, :], 0), axis=1)
    slot_span = jnp.sum(jnp.where(hit, (order // pick_count)[None, :], 0), axis=1)
    table = jnp.concatenate([slot_local, slot_span, position])
    table = jnp.pad(table, (0, -table.shape[0] % 128))

    parts = lax.axis_size("tp")
    columns = 4 if owner_count % 4 == 0 else 1
    plane = owner_count // columns
    local = plane * cap
    wide = local_heads * span_length
    tiles = row_count // block_length
    halves = 2 if tiles % 2 == 0 else 1
    tab_size = table.shape[0]
    vmem = pl.BlockSpec(memory_space=pltpu.VMEM)
    smem = pl.BlockSpec(memory_space=pltpu.SMEM)
    hbm = pl.BlockSpec(memory_space=pl.ANY)
    dma = pltpu.SemaphoreType.DMA
    V = pltpu.VMEM
    scratch = dict(
        tok=V((tiles, block_length, model), bf16),
        normed=V((tiles, block_length, model), bf16),
        st=V((store_count, passage_length, model), bf16),
        w=V((6, model, width), bf16),
        keys=V((store_count, passage_length, width), bf16),
        values_t=V((store_count, width, passage_length), bf16),
        spatial=V((tiles, block_length, width), f32),
        gated=V((tiles, block_length, width), f32),
        blend=V((tiles, block_length, width), f32),
        mom=V((tiles, block_length, 128), f32),
        mom_in=V((parts, tiles, block_length, 128), f32),
        tabs_v=V((owner_count, 1, tab_size), jnp.int32),
        tabs_s=pltpu.SMEM((owner_count, 1, tab_size), jnp.int32),
        q_own=V((span_count, span_length, width), bf16),
        qcol=[V((span_count, span_length, width), bf16)] * (columns - 1),
        qout=V((columns, plane, cap, span_length, width), bf16),
        qin=V((columns, plane, cap, span_length, width), bf16),
        rout=V((columns, plane, cap, head_dim, wide), bf16),
        lout=V((columns, plane, cap, 1, wide), f32),
        rin=[V((local, head_dim, wide), bf16)] * columns,
        lin=[V((local, 1, wide), f32)] * columns,
        mout=V((columns, span_count, head_dim, wide), bf16),
        mlout=V((columns, span_count, wide), f32),
        mid=V((columns, span_count, head_dim, wide), bf16),
        mlin=V((columns, span_count, wide), f32),
        lev=V((pick_count, span_count, wide), f32),
        wt=V((pick_count + columns, span_count, wide), f32),
        half=V((parts, row_count // parts, width), bf16),
        s=V((cap, passage_length, wide), f32),
        p=V((cap, passage_length, wide), bf16),
        tok_sem=dma((tiles,)),
        st_sem=dma((store_count,)),
        w_sem=dma((6,)),
        loc=dma((2,)),
        tab_send=dma((owner_count,)),
        tab_recv=dma((owner_count,)),
        ring_send=dma((columns, halves)),
        ring_recv=dma((columns, halves)),
        **{name: dma((columns, plane)) for name in ("qs", "qr", "rs", "rr", "ls", "lr")},
        **{name: dma((columns,)) for name in ("ms", "mr", "mls", "mlr")},
        **{name: dma((parts,)) for name in ("ts", "tr", "xs", "xr")},
    )
    by_rows = pl.pallas_call(
        functools.partial(layer_kernel, (columns, plane, parts, local_heads, cap, pick_count, halves)),
        in_specs=[smem] + [vmem] * 6 + [hbm] * 8,
        out_specs=vmem,
        out_shape=jax.ShapeDtypeStruct((row_count // parts, parts * width), bf16),
        scratch_shapes=[scratch],
        compiler_params=pltpu.CompilerParams(
            collective_id=0, has_side_effects=True, vmem_limit_bytes=60 * 2**20
        ),
        name="layer",
    )(
        table,
        table.reshape(1, tab_size),
        token_gain.reshape(1, model),
        store_gain.reshape(1, model),
        spatial_gain.reshape(1, width),
        position_bias.T,
        position_mix,
        tokens,
        store,
        query_weight,
        spatial_weight,
        key_weight,
        read_weight,
        carry_weight,
        blend_weight,
    )
    return jnp.dot(by_rows, output_weight, preferred_element_type=f32).astype(bf16)


def solution(mesh):
    in_specs = (
        P("st", None),
        P("st", None),
        P("st", None, None),
        P(),
        P(),
        P(None, "tp"),
        P(None, "tp"),
        P("tp"),
        P("tp", None, None),
        P("tp", None),
        P(None, "tp"),
        P(None, "tp"),
        P(None, "tp"),
        P(None, "tp"),
        P(),
    )
    out_specs = P(("st", "tp"), None)
    return jax.shard_map(
        per_device, mesh=mesh, in_specs=in_specs, out_specs=out_specs, check_vma=False
    )
```

time: 150 us -> 113 us (0.75)
  matrix products: 17.2 us -> 3.12 us
  Pallas kernels: 117 us -> 105 us
  local copies, waits for them, and re-layouts: 10.3 us -> 2.57 us
  blocking collectives: 2.66 us -> 0 us
    dot_general x4 -> x0, matrix products: 15.1 us -> none  [the longest x1 4.91 us: per_device(): carry_branch = jnp.dot(normed, carry_weight, preferred_element_type=f32)]
    pallas_call x3 -> x1, Pallas kernels: 117 us -> 105 us  [per_device(): pl.pallas_call(functools.partial(layer_kernel, (columns, plane, parts, lo...]
    reshape x3 -> x0, local copies, waits for them, and re-layouts: 5.74 us -> none  [the longest x2 5.41 us: per_device(): mixed_blocks.reshape(row_count, width)]
    psum x1 -> x0, blocking collectives: 2.66 us -> none  [per_device(): lax.psum((jnp.sum(spatial, axis=1), jnp.sum(spatial * spatial, axis=1)),...]
    unnamed x18 -> x3, local copies, waits for them, and re-layouts: 3.97 us -> 1.42 us
where the time goes in v2:
time: 113 us
  Pallas kernels  105 us (93%)
  matrix products  3.12 us (3%)
  local copies, waits for them, and re-layouts  2.57 us (2%)
  other arithmetic  1.91 us (2%)
    pallas_call x1, Pallas kernels, per_device(): pl.pallas_call(functools.partial(layer_kernel, (columns, plane, parts, lo...  105 us
    dot_general x1, matrix products, per_device(): jnp.dot(by_rows, output_weight, preferred_element_type=f32).astype(bf16)  3.12 us

profile of v2, /device:TPU:0, one launch (start us, length us, event | category | flops | bytes accessed | tf_op | source)
XLA Modules:
  0.0 112.8 jit_solution(2012526675669038977)
XLA Ops:
  0.0 0.0 copy-start
  0.0 0.8 sign_compare_fusion
  0.8 0.1 copy.24
  1.0 0.1 ne.74
  1.0 0.7 broadcast_remainder_fusion
  1.7 0.1 copy.25
  1.8 0.1 rem.39
  1.9 0.1 copy.26
  2.0 0.1 div.27
  2.1 0.2 convert_reduce_fusion
  2.3 0.1 select_reduce_fusion.1
  2.4 0.1 pad_add_fusion
  2.5 0.6 pad.4.own_tab
  3.1 1.4 %copy.27 = f32[4,128]{0,1:T(8,128)} copy(f32[4,128]{1,0:T(4,128)} %param.24) | data formatting | bytes 4096 | tf_op args[9]
  4.5 105.2 %layer.1 = bf16[384,512]{1,0:T(8,128)(2,1)} custom-call(s32[256]{0:T(256)} %pad.4.own_tab, s32[1,256]{1,0:T(1,128)} %bitcast.8, f32[1,2048]{1,0:T(1,128)} %bitcast.9, f32[1,2048]{1,0:T(1,128)} %bitcast.10, f32[1,256]{1,0:T(1,128)} %bitcast.11, f32[128,4]{1,0:T(8,128)} %bitcast.7, bf16[4,128,128]{2,1,0:T(8,128)(2,1)} %mix_ref.1, bf16[768,2048]{1,0:T(8,128)(2,1)} %tokens.1, ...), custom_call_target="tpu_custom_call" | custom-call | tf_op jit(solution)/shard_map/layer/pallas_call | solution.py:533
  109.7 0.0 copy-done
  109.7 3.1 %convolution_convert_fusion = bf16[384,2048]{1,0:T(8,128)(2,1)} fusion(bf16[384,512]{1,0:T(8,128)(2,1)} %layer.1, bf16[512,2048]{1,0:T(8,128)(2,1)S(1)} %copy-done), kind=kOutput, calls=%fused_computation | convolution fusion | flops 806092800 | bytes 4063232 | tf_op jit(solution)/shard_map/dot_general | solution.py:560
  (2 shorter events, 0.0 us)
Async XLA Ops:
  0.0 109.7 %copy-start = (bf16[512,2048]{1,0:T(8,128)(2,1)S(1)}, bf16[512,2048]{1,0:T(8,128)(2,1)}, u32[]{:S(2)}) copy-start(bf16[512,2048]{1,0:T(8,128)(2,1)} %param.29) | copy-start | bytes 6291460

commit v3 on v2

--- a/solution.py
+++ b/solution.py
@@ -83,6 +83,8 @@
     z = me // plane
     p = me % plane
     base = z * local
+    following = {"st": lax.rem(z + 1, columns) * plane + p}
+    group = spans // halves
 
     def each(count, f, first=0):
         def body(i, carry):
@@ -123,9 +125,8 @@
 
     def ring_copy(s, h):
         piece = pl.ds(h * (spans // halves), spans // halves)
-        where = {"st": lax.rem(z + 1, columns) * plane + p}
         send, recv = v["ring_send"].at[s, h], v["ring_recv"].at[s, h]
-        return remote(block(s).at[piece], qcol[s].at[piece], send, recv, where)
+        return remote(block(s).at[piece], qcol[s].at[piece], send, recv, following)
 
     def query_copy(s, j):
         return remote(qout.at[s, j], qin.at[s, j], v["qs"].at[s, j], v["qr"].at[s, j], mate(j))
@@ -137,12 +138,11 @@
             remote(lout.at[s, j], lin[s].at[mine], v["ls"].at[s, j], v["lr"].at[s, j], back_mate(j)),
         )
 
-    def merged_copies(s):
-        where = {"st": lax.rem(z + columns - s, columns) * plane + p}
+    def merged_copies(s, h):
         i = s - 1
         return (
-            remote(mout.at[i], mid.at[i], v["ms"].at[i], v["mr"].at[i], where),
-            remote(mlout.at[i], mlin.at[i], v["mls"].at[i], v["mlr"].at[i], where),
+            remote(mout.at[i, h], mid.at[i, h], v["ms"].at[i, h], v["mr"].at[i, h], following),
+            remote(mlout.at[i, h], mlin.at[i, h], v["mls"].at[i, h], v["mlr"].at[i, h], following),
         )
 
     def moment_copy(d):
@@ -308,13 +308,13 @@
         i = look(s, 0, 2 * slots + span * picks + k) - base
         return jnp.clip(i, 0, local - 1), (i >= 0) & (i < local)
 
-    def weigh(s, more):
-        def one(span):
+    def weigh(s, h, more):
+        def one(i):
             for k in range(picks):
-                i, inside = source(s, span, k)
-                v["lev"][k, pl.ds(span, 1)] = jnp.where(inside, lin[s][i], far)
-
-        each(spans, one)
+                at, inside = source(s, h * group + i, k)
+                v["lev"][k, pl.ds(i, 1)] = jnp.where(inside, lin[s][at], far)
+
+        each(group, one)
         levels = [v["lev"][k] for k in range(picks)] + more
         top = functools.reduce(jnp.maximum, levels)
         ws = [jnp.exp(level - top) for level in levels]
@@ -323,11 +323,11 @@
             v["wt"][k] = w / total
         return top + jnp.log(total)
 
-    def summed(s, span, more):
-        at = pl.ds(span, 1)
-        terms = [v["wt"][k, at] * rin[s][source(s, span, k)[0]].astype(f32) for k in range(picks)]
+    def summed(s, h, i, more):
+        at = pl.ds(i, 1)
+        terms = [v["wt"][k, at] * rin[s][source(s, h * group + i, k)[0]].astype(f32) for k in range(picks)]
         for k, ref in enumerate(more):
-            terms.append(v["wt"][picks + k, at] * ref[span].astype(f32))
+            terms.append(v["wt"][picks + k, at] * ref[i].astype(f32))
         return sum(terms)
 
     def wait_results(s):
@@ -337,16 +337,27 @@
 
         each(plane, one, 1)
 
+    def arrived(s, h):
+        if (s if s else columns) < 2:
+            return [], []
+        i = (s if s else columns) - 2
+        for copy in merged_copies(i + 1, h):
+            copy.wait_recv()
+        return [mlin[i, h]], [mid.at[i, h]]
+
     def merge(s):
         wait_results(s)
-        mlout[s - 1] = weigh(s, [])
-
-        def one(span):
-            mout[s - 1, span] = summed(s, span, []).astype(bf16)
-
-        each(spans, one)
-        for copy in merged_copies(s):
-            copy.start()
+        for d in range(1, halves + 1):
+            h = lax.rem(side + d, halves)
+            levels, blocks = arrived(s, h)
+            mlout[s - 1, h] = weigh(s, h, levels)
+
+            def one(i):
+                mout[s - 1, h, i] = summed(s, h, i, blocks).astype(bf16)
+
+            each(group, one)
+            for copy in merged_copies(s, h):
+                copy.start()
 
     own_copy.wait()
     weight_copy(2).wait()
@@ -369,30 +380,31 @@
             attention(s - 1)
         if s == 2:
             spatial_rest()
+    for s in range(1, columns - 1):
+        merge(s)
+        if s == 1:
+            attention(0, False)
+            attention(columns - 1)
+            each(plane, lambda j: send_results(0, j), 1)
     if columns > 1:
-        attention(columns - 1)
-    attention(0)
-    for s in range(1, columns):
-        merge(s)
+        merge(columns - 1)
     wait_results(0)
-    for s in range(1, columns):
-        for copy in merged_copies(s):
-            copy.wait_recv()
-
-    share = spans // parts
-    weigh(0, [mlin[s - 1] for s in range(1, columns)])
+
     lanes = pl.ds(pl.multiple_of(side * width, width), width)
 
-    def final(first, to):
+    def final(h, to):
+        levels, blocks = arrived(0, h)
+        weigh(0, h, levels)
+
         def one(i):
-            span = first + i
-            memory = summed(0, span, [mid.at[s - 1] for s in range(1, columns)]).T
-            memory = jnp.concatenate([memory[h * length : (h + 1) * length] for h in range(heads)], axis=1)
+            span = h * group + i
+            memory = summed(0, h, i, blocks).T
+            memory = jnp.concatenate([memory[c * length : (c + 1) * length] for c in range(heads)], axis=1)
             at = pl.ds(pl.multiple_of(lax.rem(span, per) * length, length), length)
             t = span // per
             to(i, (v["gated"][t, at] + v["blend"][t, at] * memory).astype(bf16))
 
-        each(share, one)
+        each(group, one)
 
     def half_copy(d):
         i = d - 1
@@ -406,13 +418,13 @@
         def keep(i, value):
             half[d - 1, rows_of(i)] = value
 
-        final(lax.rem(side + d, parts) * share, keep)
+        final(lax.rem(side + d, parts), keep)
         half_copy(d).start()
 
     def keep_own(i, value):
         out_ref[rows_of(i), lanes] = value
 
-    final(side * share, keep_own)
+    final(side, keep_own)
 
     for d in range(1, parts):
         half_copy(d).wait()
@@ -430,8 +442,9 @@
 
         each(plane, done, 1)
     for s in range(1, columns):
-        for copy in merged_copies(s):
-            copy.wait_send()
+        for h in range(halves):
+            for copy in merged_copies(s, h):
+                copy.wait_send()
 
 
 def per_device(
@@ -480,7 +493,8 @@
     local = plane * cap
     wide = local_heads * span_length
     tiles = row_count // block_length
-    halves = 2 if tiles % 2 == 0 else 1
+    halves = parts
+    group = span_count // halves
     tab_size = table.shape[0]
     vmem = pl.BlockSpec(memory_space=pltpu.VMEM)
     smem = pl.BlockSpec(memory_space=pltpu.SMEM)
@@ -509,12 +523,12 @@
         lout=V((columns, plane, cap, 1, wide), f32),
         rin=[V((local, head_dim, wide), bf16)] * columns,
         lin=[V((local, 1, wide), f32)] * columns,
-        mout=V((columns, span_count, head_dim, wide), bf16),
-        mlout=V((columns, span_count, wide), f32),
-        mid=V((columns, span_count, head_dim, wide), bf16),
-        mlin=V((columns, span_count, wide), f32),
-        lev=V((pick_count, span_count, wide), f32),
-        wt=V((pick_count + columns, span_count, wide), f32),
+        mout=V((columns, halves, group, head_dim, wide), bf16),
+        mlout=V((columns, halves, group, wide), f32),
+        mid=V((columns, halves, group, head_dim, wide), bf16),
+        mlin=V((columns, halves, group, wide), f32),
+        lev=V((pick_count, group, wide), f32),
+        wt=V((pick_count + 1, group, wide), f32),
         half=V((parts, row_count // parts, width), bf16),
         s=V((cap, passage_length, wide), f32),
         p=V((cap, passage_length, wide), bf16),
@@ -527,7 +541,7 @@
         ring_send=dma((columns, halves)),
         ring_recv=dma((columns, halves)),
         **{name: dma((columns, plane)) for name in ("qs", "qr", "rs", "rr", "ls", "lr")},
-        **{name: dma((columns,)) for name in ("ms", "mr", "mls", "mlr")},
+        **{name: dma((columns, halves)) for name in ("ms", "mr", "mls", "mlr")},
         **{name: dma((parts,)) for name in ("ts", "tr", "xs", "xr")},
     )
     by_rows = pl.pallas_call(

time: 113 us -> 99.3 us (0.88)
  Pallas kernels: 105 us -> 90.7 us
    pallas_call x1, Pallas kernels: 105 us -> 90.7 us  [per_device(): pl.pallas_call(functools.partial(layer_kernel, (columns, plane, parts, lo...]
where the time goes in v3:
time: 99.3 us; the launch traced here: 98.3 us
  Pallas kernels  90.7 us (91%)
  matrix products  3.12 us (3%)
  local copies, waits for them, and re-layouts  2.57 us (3%)
  other arithmetic  1.91 us (2%)
    pallas_call x1, Pallas kernels, per_device(): pl.pallas_call(functools.partial(layer_kernel, (columns, plane, parts, lo...  90.7 us
    dot_general x1, matrix products, per_device(): jnp.dot(by_rows, output_weight, preferred_element_type=f32).astype(bf16)  3.12 us

profile of v3, /device:TPU:0, one launch (start us, length us, event | category | flops | bytes accessed | tf_op | source)
XLA Modules:
  0.0 98.3 jit_solution(11999249165749962651)
XLA Ops:
  0.0 0.0 copy-start
  0.0 0.8 sign_compare_fusion
  0.8 0.1 copy.24
  1.0 0.1 ne.74
  1.0 0.7 broadcast_remainder_fusion
  1.7 0.1 copy.25
  1.8 0.1 rem.39
  1.9 0.1 copy.26
  2.0 0.1 div.27
  2.1 0.2 convert_reduce_fusion
  2.3 0.1 select_reduce_fusion.1
  2.4 0.1 pad_add_fusion
  2.5 0.6 pad.4.own_tab
  3.1 1.4 %copy.27 = f32[4,128]{0,1:T(8,128)} copy(f32[4,128]{1,0:T(4,128)} %param.24) | data formatting | bytes 4096 | tf_op args[9]
  4.5 90.7 %layer.1 = bf16[384,512]{1,0:T(8,128)(2,1)} custom-call(s32[256]{0:T(256)} %pad.4.own_tab, s32[1,256]{1,0:T(1,128)} %bitcast.8, f32[1,2048]{1,0:T(1,128)} %bitcast.9, f32[1,2048]{1,0:T(1,128)} %bitcast.10, f32[1,256]{1,0:T(1,128)} %bitcast.11, f32[128,4]{1,0:T(8,128)} %bitcast.7, bf16[4,128,128]{2,1,0:T(8,128)(2,1)} %mix_ref.1, bf16[768,2048]{1,0:T(8,128)(2,1)} %tokens.1, ...), custom_call_target="tpu_custom_call" | custom-call | tf_op jit(solution)/shard_map/layer/pallas_call | solution.py:547
  95.2 0.0 copy-done
  95.2 3.1 %convolution_convert_fusion = bf16[384,2048]{1,0:T(8,128)(2,1)} fusion(bf16[384,512]{1,0:T(8,128)(2,1)} %layer.1, bf16[512,2048]{1,0:T(8,128)(2,1)S(1)} %copy-done), kind=kOutput, calls=%fused_computation | convolution fusion | flops 806092800 | bytes 4063232 | tf_op jit(solution)/shard_map/dot_general | solution.py:574
  (2 shorter events, 0.0 us)
Async XLA Ops:
  0.0 95.2 %copy-start = (bf16[512,2048]{1,0:T(8,128)(2,1)S(1)}, bf16[512,2048]{1,0:T(8,128)(2,1)}, u32[]{:S(2)}) copy-start(bf16[512,2048]{1,0:T(8,128)(2,1)} %param.29) | copy-start | bytes 6291460

commit v4 on v3

--- a/solution.py
+++ b/solution.py
@@ -43,10 +43,46 @@
     return 0.5 * x * (1.0 + lax.erf(x * 0.5**0.5))
 
 
+def fill_table(ids_ref, tab_ref, n, cap, count):
+    picks, spans = ids_ref.shape
+    requests = spans * picks
+    i32 = jnp.int32
+    wide = tab_ref.shape[1] - 2 * (-(-n * cap // 128) * 128)
+    lane = lax.broadcasted_iota(i32, (picks, wide), 1)
+    pick = lax.broadcasted_iota(i32, (picks, wide), 0)
+    spread = jnp.zeros((picks, wide), i32)
+    for s in range(spans):
+        spread = spread + jnp.where(lane == s * picks + pick, ids_ref[:, s : s + 1], 0)
+    ids = sum(spread[k : k + 1] for k in range(picks))
+    lane = lane[0:1]
+    owner = jnp.zeros((1, wide), i32)
+    for o in range(1, n):
+        owner = owner + jnp.where(ids >= o * count, 1, 0)
+    inside = ids - owner * count
+    span = jnp.zeros((1, wide), i32)
+    for s in range(1, spans):
+        span = span + jnp.where(lane >= s * picks, 1, 0)
+    owner = jnp.where(lane < requests, owner, n)
+
+    def down(row):
+        return jnp.broadcast_to(row, (wide, wide)).T
+
+    row_of = lax.broadcasted_iota(i32, (wide, wide), 0)
+    lane_of = lax.broadcasted_iota(i32, (wide, wide), 1)
+    earlier = (down(owner) == owner) & (row_of < lane_of)
+    position = owner * cap + jnp.sum(jnp.where(earlier, 1, 0), axis=0, keepdims=True)
+    place, inside, span = down(position), down(inside), down(span)
+    section = (tab_ref.shape[1] - wide) // 2
+    for b in range(0, section, wide):
+        hit = (place == lane_of + b) & (row_of < requests)
+        tab_ref[:, b : b + wide] = jnp.sum(jnp.where(hit, inside, 0), axis=0, keepdims=True)
+        tab_ref[:, section + b : section + b + wide] = jnp.sum(jnp.where(hit, span, 0), axis=0, keepdims=True)
+    tab_ref[:, 2 * section :] = position
+
+
 def layer_kernel(
     sizes,
-    own_tab,
-    tab_ref,
+    ids_ref,
     token_gain,
     store_gain,
     spatial_gain,
@@ -67,6 +103,7 @@
     q_own, qcol, qout, qin = v["q_own"], v["qcol"], v["qout"], v["qin"]
     rout, lout, rin, lin = v["rout"], v["lout"], v["rin"], v["lin"]
     mout, mlout, mid, mlin, half = v["mout"], v["mlout"], v["mid"], v["mlin"], v["half"]
+    tab_ref, own_tab = v["tab"], v["own_tab"]
     tabs_v, tabs_s, normed = v["tabs_v"], v["tabs_s"], v["normed"]
     keys, values_t, w_ref = v["keys"], v["values_t"], v["w"]
     n = columns * plane
@@ -77,6 +114,7 @@
     dim = width // heads
     scale = dim ** (-0.5)
     slots = n * cap
+    section = -(-slots // 128) * 128
     local = plane * cap
     me = lax.axis_index("st")
     side = lax.axis_index("tp")
@@ -154,9 +192,6 @@
 
     weight_copy(0).start()
     each(tiles, lambda i: token_copy(i).start())
-    for i in range(1, 6):
-        weight_copy(i).start()
-    each(store_count, lambda i: store_copy(i).start())
 
     barrier = pltpu.get_barrier_semaphore()
 
@@ -167,6 +202,7 @@
     for d in range(1, parts):
         pl.semaphore_signal(barrier, inc=1, device_id=other(d), device_id_type=MESH)
 
+    fill_table(ids_ref, tab_ref, n, cap, store_count)
     weight_copy(0).wait()
 
     def query(i):
@@ -180,19 +216,25 @@
     for h in range(halves):
         each(tiles * (h + 1) // halves, query, tiles * h // halves)
         if h == 0:
+            table_copy = pltpu.make_async_copy(tab_ref, own_tab, v["loc"].at[2])
+            table_copy.start()
             pl.semaphore_wait(barrier, n - 1 + parts - 1)
         if columns > 1:
             ring_copy(0, h).start()
     each(n, lambda d: tab_copy(d).start(), 1)
     own_copy = pltpu.make_async_copy(tab_ref, tabs_v.at[me], v["loc"].at[0])
     own_copy.start()
+    for i in range(1, 6):
+        weight_copy(i).start()
+    each(store_count, lambda i: store_copy(i).start())
+    table_copy.wait()
 
     def select(s):
         def pick(j):
             o = z * plane + lax.rem(p + j, plane)
             for c in range(cap):
-                i = slots + o * cap + c
-                span = own_tab[i] if s == 0 else look(s, 0, i)
+                i = section + o * cap + c
+                span = own_tab[0, i] if s == 0 else look(s, 0, i)
                 qout[s, j, c] = block(s)[span]
 
         each(plane, pick, 1)
@@ -235,9 +277,10 @@
             spread = mom[:, 64:65] - mean * mean
             x = (v["spatial"][i] - mean) * lax.rsqrt(spread + norm_eps) * spatial_gain[...]
             x = x.astype(bf16)
+            bias = jnp.concatenate([bias_ref[...]] * (-(-8 // heads)), axis=0).T
             mixed = [
                 jnp.dot(mix_ref[h], x[:, h * dim : (h + 1) * dim], preferred_element_type=f32)
-                + bias_ref[:, h : h + 1]
+                + bias[:, h : h + 1]
                 for h in range(heads)
             ]
             mixed = jnp.concatenate(mixed, axis=1)
@@ -299,13 +342,13 @@
             rin[s][p * cap + c] = value
             lin[s][p * cap + c] = level
 
-        here = [block(s)[look(s, 0, slots + mine + c)] for c in range(cap)]
+        here = [block(s)[look(s, 0, section + mine + c)] for c in range(cap)]
         if send and plane > 1:
             send_results(s, plane - 1)
         attend(here, [look(s, 0, mine + c) for c in range(cap)], put_here)
 
     def source(s, span, k):
-        i = look(s, 0, 2 * slots + span * picks + k) - base
+        i = look(s, 0, 2 * section + span * picks + k) - base
         return jnp.clip(i, 0, local - 1), (i >= 0) & (i < local)
 
     def weigh(s, h, more):
@@ -476,17 +519,6 @@
     cap = max(1, 2 * requests // owner_count)
     slots = owner_count * cap
 
-    flat_ids = route_ids.reshape(requests)
-    owner = flat_ids // store_count
-    order = jnp.arange(requests, dtype=jnp.int32)
-    earlier = (owner[:, None] == owner[None, :]) & (order[None, :] < order[:, None])
-    position = owner * cap + jnp.sum(earlier.astype(jnp.int32), axis=1)
-    hit = position[None, :] == jnp.arange(slots, dtype=jnp.int32)[:, None]
-    slot_local = jnp.sum(jnp.where(hit, (flat_ids % store_count)[None, :], 0), axis=1)
-    slot_span = jnp.sum(jnp.where(hit, (order // pick_count)[None, :], 0), axis=1)
-    table = jnp.concatenate([slot_local, slot_span, position])
-    table = jnp.pad(table, (0, -table.shape[0] % 128))
-
     parts = lax.axis_size("tp")
     columns = 4 if owner_count % 4 == 0 else 1
     plane = owner_count // columns
@@ -495,10 +527,9 @@
     tiles = row_count // block_length
     halves = parts
     group = span_count // halves
-    tab_size = table.shape[0]
+    tab_size = 2 * (-(-owner_count * cap // 128) * 128) + (-(-requests // 128) * 128)
     vmem = pl.BlockSpec(memory_space=pltpu.VMEM)
-    smem = pl.BlockSpec(memory_space=pltpu.SMEM)
-    hbm = pl.BlockSpec(memory_space=pl.ANY)
+    hbm = pl.BlockSpec(memory_space=pltpu.HBM)
     dma = pltpu.SemaphoreType.DMA
     V = pltpu.VMEM
     scratch = dict(
@@ -513,6 +544,8 @@
         blend=V((tiles, block_length, width), f32),
         mom=V((tiles, block_length, 128), f32),
         mom_in=V((parts, tiles, block_length, 128), f32),
+        tab=V((1, tab_size), jnp.int32),
+        own_tab=pltpu.SMEM((1, tab_size), jnp.int32),
         tabs_v=V((owner_count, 1, tab_size), jnp.int32),
         tabs_s=pltpu.SMEM((owner_count, 1, tab_size), jnp.int32),
         q_own=V((span_count, span_length, width), bf16),
@@ -535,7 +568,7 @@
         tok_sem=dma((tiles,)),
         st_sem=dma((store_count,)),
         w_sem=dma((6,)),
-        loc=dma((2,)),
+        loc=dma((3,)),
         tab_send=dma((owner_count,)),
         tab_recv=dma((owner_count,)),
         ring_send=dma((columns, halves)),
@@ -546,21 +579,20 @@
     )
     by_rows = pl.pallas_call(
         functools.partial(layer_kernel, (columns, plane, parts, local_heads, cap, pick_count, halves)),
-        in_specs=[smem] + [vmem] * 6 + [hbm] * 8,
+        in_specs=[vmem] * 6 + [hbm] * 8,
         out_specs=vmem,
         out_shape=jax.ShapeDtypeStruct((row_count // parts, parts * width), bf16),
         scratch_shapes=[scratch],
         compiler_params=pltpu.CompilerParams(
-            collective_id=0, has_side_effects=True, vmem_limit_bytes=60 * 2**20
+            collective_id=0, has_side_effects=True, vmem_limit_bytes=53 * 2**20
         ),
         name="layer",
     )(
-        table,
-        table.reshape(1, tab_size),
+        route_ids.T,
         token_gain.reshape(1, model),
         store_gain.reshape(1, model),
         spatial_gain.reshape(1, width),
-        position_bias.T,
+        position_bias,
         position_mix,
         tokens,
         store,

time: 99.3 us -> 98 us (0.987)
  local copies, waits for them, and re-layouts: 2.57 us -> 4.49 us
  other arithmetic: 1.91 us -> 0 us
    unnamed x3 -> x14, local copies, waits for them, and re-layouts: 1.42 us -> 4.49 us
where the time goes in v4:
time: 98 us; the launch traced here: 97.1 us
  Pallas kernels  90.4 us (92%)
  local copies, waits for them, and re-layouts  4.49 us (5%)
  matrix products  2.16 us (2%)
    pallas_call x1, Pallas kernels, per_device(): pl.pallas_call(functools.partial(layer_kernel, (columns, plane, parts, lo...  90.4 us
    unnamed x14, local copies, waits for them, and re-layouts  4.49 us
    dot_general x1, matrix products, per_device(): jnp.dot(by_rows, output_weight, preferred_element_type=f32).astype(bf16)  2.16 us

profile of v4, /device:TPU:0, one launch (start us, length us, event | category | flops | bytes accessed | tf_op | source)
XLA Modules:
  0.0 97.1 jit_solution(10500805459124098230)
XLA Ops:
  0.0 0.0 copy-start
  0.0 0.0 copy-start.1
  0.0 1.1 %copy-done.1 = bf16[4,128,128]{2,1,0:T(8,128)(2,1)S(1)} copy-done((bf16[4,128,128]{2,1,0:T(8,128)(2,1)S(1)}, bf16[4,128,128]{2,1,0:T(8,128)(2,1)}, u32[]{:S(2)}) %copy-start.1) | copy-done | bytes 131096
  1.1 0.0 copy-start.2
  1.1 0.7 copy-done.2
  1.8 0.0 copy-start.3
  1.8 0.7 copy-done.3
  2.5 0.0 copy-start.4
  2.5 0.7 copy-done.4
  3.1 0.0 copy-start.5
  3.1 0.7 copy-done.5
  3.8 0.0 copy-start.6
  3.8 0.7 copy-done.6
  4.5 90.4 %layer.1 = bf16[384,512]{1,0:T(8,128)(2,1)S(1)} custom-call(s32[4,12]{1,0:T(4,128)S(1)} %bitcast.8, f32[1,2048]{1,0:T(1,128)S(1)} %bitcast.6, f32[1,2048]{1,0:T(1,128)S(1)} %bitcast.7, f32[1,256]{1,0:T(1,128)S(1)} %bitcast.9, f32[4,128]{1,0:T(4,128)S(1)} %copy-done.5, bf16[4,128,128]{2,1,0:T(8,128)(2,1)S(1)} %copy-done.1, bf16[768,2048]{1,0:T(8,128)(2,1)} %tokens.1, ...), custom_call_target="tpu_custom_call" | custom-call | tf_op jit(solution)/shard_map/layer/pallas_call | solution.py:580
  94.9 0.0 copy-done
  94.9 2.2 %convolution_convert_fusion = bf16[384,2048]{1,0:T(8,128)(2,1)} fusion(bf16[384,512]{1,0:T(8,128)(2,1)S(1)} %layer.1, bf16[512,2048]{1,0:T(8,128)(2,1)S(1)} %copy-done), kind=kOutput, calls=%fused_computation | convolution fusion | flops 806092800 | bytes 4063232 | tf_op jit(solution)/shard_map/dot_general | solution.py:606
Async XLA Ops:
  0.0 94.9 %copy-start = (bf16[512,2048]{1,0:T(8,128)(2,1)S(1)}, bf16[512,2048]{1,0:T(8,128)(2,1)}, u32[]{:S(2)}) copy-start(bf16[512,2048]{1,0:T(8,128)(2,1)} %param.29) | copy-start | bytes 6291460
  0.0 1.1 %copy-start.1 = (bf16[4,128,128]{2,1,0:T(8,128)(2,1)S(1)}, bf16[4,128,128]{2,1,0:T(8,128)(2,1)}, u32[]{:S(2)}) copy-start(bf16[4,128,128]{2,1,0:T(8,128)(2,1)} %mix_ref.1) | copy-start | bytes 393220
  1.1 0.7 copy-start.2
  1.8 0.7 copy-start.3
  2.5 0.7 copy-start.4
  3.1 0.7 copy-start.5
  3.8 0.7 copy-start.6

commit v5 on v4

--- a/solution.py
+++ b/solution.py
@@ -82,12 +82,12 @@
 
 def layer_kernel(
     sizes,
-    ids_ref,
-    token_gain,
-    store_gain,
-    spatial_gain,
-    bias_ref,
-    mix_ref,
+    ids_in,
+    token_gain_in,
+    store_gain_in,
+    spatial_gain_in,
+    bias_in,
+    mix_in,
     tokens,
     store,
     wq,
@@ -104,6 +104,8 @@
     rout, lout, rin, lin = v["rout"], v["lout"], v["rin"], v["lin"]
     mout, mlout, mid, mlin, half = v["mout"], v["mlout"], v["mid"], v["mlin"], v["half"]
     tab_ref, own_tab = v["tab"], v["own_tab"]
+    small = (ids_in, token_gain_in, store_gain_in, spatial_gain_in, bias_in, mix_in)
+    ids_ref, token_gain, store_gain, spatial_gain, bias_ref, mix_ref = v["small"]
     tabs_v, tabs_s, normed = v["tabs_v"], v["tabs_s"], v["normed"]
     keys, values_t, w_ref = v["keys"], v["values_t"], v["w"]
     n = columns * plane
@@ -190,8 +192,15 @@
         row = lax.rem(z + columns - s, columns) * plane + lax.rem(p + plane - j, plane)
         return tabs_s[row, 0, i]
 
+    def small_copy(i):
+        return pltpu.make_async_copy(small[i], v["small"][i], v["small_sem"].at[i])
+
+    small_copy(0).start()
+    small_copy(1).start()
     weight_copy(0).start()
     each(tiles, lambda i: token_copy(i).start())
+    for i in range(2, 6):
+        small_copy(i).start()
 
     barrier = pltpu.get_barrier_semaphore()
 
@@ -202,7 +211,9 @@
     for d in range(1, parts):
         pl.semaphore_signal(barrier, inc=1, device_id=other(d), device_id_type=MESH)
 
+    small_copy(0).wait()
     fill_table(ids_ref, tab_ref, n, cap, store_count)
+    small_copy(1).wait()
     weight_copy(0).wait()
 
     def query(i):
@@ -227,6 +238,8 @@
     for i in range(1, 6):
         weight_copy(i).start()
     each(store_count, lambda i: store_copy(i).start())
+    for i in range(2, 6):
+        small_copy(i).wait()
     table_copy.wait()
 
     def select(s):
@@ -405,24 +418,29 @@
     own_copy.wait()
     weight_copy(2).wait()
     weight_copy(3).wait()
-    steps = max(columns - 1, 1)
-    cut = [store_count * min(i, 2) // 2 for i in range(steps + 1)] if steps > 1 else [0, store_count]
+    cuts = [store_count * part // 24 for part in (0, 3, 8, 14, 20, 24)]
+    if columns == 1:
+        each(store_count, project)
     for s in range(1, columns):
-        each(cut[s], project, cut[s - 1])
-        if s == 1:
-            each(n, lambda d: tab_copy(d).wait_recv(), 1)
-            to_smem = pltpu.make_async_copy(tabs_v, tabs_s, v["loc"].at[1])
-            to_smem.start()
-            to_smem.wait()
         for h in range(halves):
+            k = (s - 1) * halves + h
+            if k + 1 < len(cuts):
+                each(cuts[k + 1], project, cuts[k])
+            if k == 0:
+                each(n, lambda d: tab_copy(d).wait_recv(), 1)
+                to_smem = pltpu.make_async_copy(tabs_v, tabs_s, v["loc"].at[1])
+                to_smem.start()
+                to_smem.wait()
+            if s == columns - 1 and h == 0:
+                for done in range(1, s - 1):
+                    attention(done)
             ring_copy(s - 1, h).wait_recv()
             if s < columns - 1:
                 ring_copy(s, h).start()
         select(s)
-        if s > 1:
-            attention(s - 1)
-        if s == 2:
-            spatial_rest()
+    spatial_rest()
+    if columns > 1:
+        attention(columns - 2)
     for s in range(1, columns - 1):
         merge(s)
         if s == 1:
@@ -544,6 +562,15 @@
         blend=V((tiles, block_length, width), f32),
         mom=V((tiles, block_length, 128), f32),
         mom_in=V((parts, tiles, block_length, 128), f32),
+        small=[
+            V((pick_count, span_count), jnp.int32),
+            V((1, model), f32),
+            V((1, model), f32),
+            V((1, width), f32),
+            V((local_heads, block_length), f32),
+            V((local_heads, block_length, block_length), bf16),
+        ],
+        small_sem=dma((6,)),
         tab=V((1, tab_size), jnp.int32),
         own_tab=pltpu.SMEM((1, tab_size), jnp.int32),
         tabs_v=V((owner_count, 1, tab_size), jnp.int32),
@@ -579,12 +606,12 @@
     )
     by_rows = pl.pallas_call(
         functools.partial(layer_kernel, (columns, plane, parts, local_heads, cap, pick_count, halves)),
-        in_specs=[vmem] * 6 + [hbm] * 8,
+        in_specs=[hbm] * 14,
         out_specs=vmem,
         out_shape=jax.ShapeDtypeStruct((row_count // parts, parts * width), bf16),
         scratch_shapes=[scratch],
         compiler_params=pltpu.CompilerParams(
-            collective_id=0, has_side_effects=True, vmem_limit_bytes=53 * 2**20
+            collective_id=0, has_side_effects=True, vmem_limit_bytes=60 * 2**20
         ),
         name="layer",
     )(

time: 98 us -> 94.3 us (0.962)
  local copies, waits for them, and re-layouts: 4.49 us -> 0.01 us
    unnamed x14 -> x2, local copies, waits for them, and re-layouts: 4.49 us -> 0.01 us
where the time goes in v5:
time: 94.3 us; the launch traced here: 94.2 us
  Pallas kernels  91 us (97%)
  matrix products  3.12 us (3%)
    pallas_call x1, Pallas kernels, per_device(): pl.pallas_call(functools.partial(layer_kernel, (columns, plane, parts, lo...  91 us
    dot_general x1, matrix products, per_device(): jnp.dot(by_rows, output_weight, preferred_element_type=f32).astype(bf16)  3.12 us

profile of v5, /device:TPU:0, one launch (start us, length us, event | category | flops | bytes accessed | tf_op | source)
XLA Modules:
  0.0 94.2 jit_solution(8148388559663331199)
XLA Ops:
  0.0 0.0 copy-start
  0.0 91.0 %layer.1 = bf16[384,512]{1,0:T(8,128)(2,1)} custom-call(s32[4,12]{1,0:T(4,128)} %bitcast.8, f32[1,2048]{1,0:T(1,128)} %bitcast.6, f32[1,2048]{1,0:T(1,128)} %bitcast.7, f32[1,256]{1,0:T(1,128)} %bitcast.9, f32[4,128]{1,0:T(4,128)} %bias_in.1, bf16[4,128,128]{2,1,0:T(8,128)(2,1)} %mix_in.1, bf16[768,2048]{1,0:T(8,128)(2,1)} %tokens.1, ...), custom_call_target="tpu_custom_call" | custom-call | tf_op jit(solution)/shard_map/layer/pallas_call | solution.py:607
  91.0 0.0 copy-done
  91.0 3.1 %convolution_convert_fusion = bf16[384,2048]{1,0:T(8,128)(2,1)} fusion(bf16[384,512]{1,0:T(8,128)(2,1)} %layer.1, bf16[512,2048]{1,0:T(8,128)(2,1)S(1)} %copy-done), kind=kOutput, calls=%fused_computation | convolution fusion | flops 806092800 | bytes 4063232 | tf_op jit(solution)/shard_map/dot_general | solution.py:633
Async XLA Ops:
  0.0 91.0 %copy-start = (bf16[512,2048]{1,0:T(8,128)(2,1)S(1)}, bf16[512,2048]{1,0:T(8,128)(2,1)}, u32[]{:S(2)}) copy-start(bf16[512,2048]{1,0:T(8,128)(2,1)} %param.29) | copy-start | bytes 6291460

commit v6 on v5

--- a/solution.py
+++ b/solution.py
@@ -269,11 +269,20 @@
     for d in range(1, parts):
         moment_copy(d).start()
 
+    batch = 2 if store_count % 2 == 0 else 1
+    passage = keys.shape[1]
+
     def project(i):
-        store_copy(i).wait()
-        rows = normed_rows(v["st"][i], store_gain[...])
-        keys[i] = jnp.dot(rows, w_ref[2], preferred_element_type=f32).astype(bf16)
-        values_t[i] = jnp.dot(rows, w_ref[3], preferred_element_type=f32).T.astype(bf16)
+        for c in range(batch):
+            store_copy(i * batch + c).wait()
+        rows = [normed_rows(v["st"][i * batch + c], store_gain[...]) for c in range(batch)]
+        rows = jnp.concatenate(rows, axis=0)
+        k = jnp.dot(rows, w_ref[2], preferred_element_type=f32).astype(bf16)
+        x = jnp.dot(rows, w_ref[3], preferred_element_type=f32)
+        for c in range(batch):
+            at = slice(c * passage, (c + 1) * passage)
+            keys[i * batch + c] = k[at]
+            values_t[i * batch + c] = x[at].T.astype(bf16)
 
     def spatial_rest():
         for d in range(1, parts):
@@ -418,9 +427,9 @@
     own_copy.wait()
     weight_copy(2).wait()
     weight_copy(3).wait()
-    cuts = [store_count * part // 24 for part in (0, 3, 8, 14, 20, 24)]
+    cuts = [store_count // batch * part // 12 for part in (0, 1, 4, 7, 10, 12)]
     if columns == 1:
-        each(store_count, project)
+        each(store_count // batch, project)
     for s in range(1, columns):
         for h in range(halves):
             k = (s - 1) * halves + h
@@ -550,6 +559,7 @@
     hbm = pl.BlockSpec(memory_space=pltpu.HBM)
     dma = pltpu.SemaphoreType.DMA
     V = pltpu.VMEM
+    in_hbm = lambda x: pltpu.with_memory_space_constraint(x, pltpu.HBM)
     scratch = dict(
         tok=V((tiles, block_length, model), bf16),
         normed=V((tiles, block_length, model), bf16),
@@ -611,16 +621,16 @@
         out_shape=jax.ShapeDtypeStruct((row_count // parts, parts * width), bf16),
         scratch_shapes=[scratch],
         compiler_params=pltpu.CompilerParams(
-            collective_id=0, has_side_effects=True, vmem_limit_bytes=60 * 2**20
+            collective_id=0, has_side_effects=True, vmem_limit_bytes=53 * 2**20
         ),
         name="layer",
     )(
-        route_ids.T,
-        token_gain.reshape(1, model),
-        store_gain.reshape(1, model),
-        spatial_gain.reshape(1, width),
-        position_bias,
-        position_mix,
+        in_hbm(route_ids.T),
+        in_hbm(token_gain.reshape(1, model)),
+        in_hbm(store_gain.reshape(1, model)),
+        in_hbm(spatial_gain.reshape(1, width)),
+        in_hbm(position_bias),
+        in_hbm(position_mix),
         tokens,
         store,
         query_weight,

time: 94.3 us -> 91.9 us (0.975)
  Pallas kernels: 91 us -> 89.6 us
  matrix products: 3.12 us -> 2.13 us
    pallas_call x1, Pallas kernels: 91 us -> 89.6 us  [per_device(): pl.pallas_call(functools.partial(layer_kernel, (columns, plane, parts, lo...]
    dot_general x1, matrix products: 3.12 us -> 2.13 us  [per_device(): jnp.dot(by_rows, output_weight, preferred_element_type=f32).astype(bf16)]
where the time goes in v6:
time: 91.9 us; the launch traced here: 91.8 us
  Pallas kernels  89.6 us (97%)
  matrix products  2.13 us (2%)
    pallas_call x1, Pallas kernels, per_device(): pl.pallas_call(functools.partial(layer_kernel, (columns, plane, parts, lo...  89.6 us
    dot_general x1, matrix products, per_device(): jnp.dot(by_rows, output_weight, preferred_element_type=f32).astype(bf16)  2.13 us

profile of v6, /device:TPU:0, one launch (start us, length us, event | category | flops | bytes accessed | tf_op | source)
XLA Modules:
  0.0 91.8 jit_solution(3793357418064375593)
XLA Ops:
  0.0 0.0 copy-start
  0.0 89.6 %layer.1 = bf16[384,512]{1,0:T(8,128)(2,1)S(1)} custom-call(s32[4,12]{1,0:T(4,128)} %bitcast.8, f32[1,2048]{1,0:T(1,128)} %bitcast.6, f32[1,2048]{1,0:T(1,128)} %bitcast.7, f32[1,256]{1,0:T(1,128)} %bitcast.9, f32[4,128]{1,0:T(4,128)} %bias_in.1, bf16[4,128,128]{2,1,0:T(8,128)(2,1)} %mix_in.1, bf16[768,2048]{1,0:T(8,128)(2,1)} %tokens.1, ...), custom_call_target="tpu_custom_call" | custom-call | tf_op jit(solution)/shard_map/layer/pallas_call | solution.py:617
  89.6 0.0 copy-done
  89.6 2.1 %convolution_convert_fusion = bf16[384,2048]{1,0:T(8,128)(2,1)} fusion(bf16[384,512]{1,0:T(8,128)(2,1)S(1)} %layer.1, bf16[512,2048]{1,0:T(8,128)(2,1)S(1)} %copy-done), kind=kOutput, calls=%fused_computation | convolution fusion | flops 806092800 | bytes 4063232 | tf_op jit(solution)/shard_map/dot_general | solution.py:643
Async XLA Ops:
  0.0 89.6 %copy-start = (bf16[512,2048]{1,0:T(8,128)(2,1)S(1)}, bf16[512,2048]{1,0:T(8,128)(2,1)}, u32[]{:S(2)}) copy-start(bf16[512,2048]{1,0:T(8,128)(2,1)} %param.29) | copy-start | bytes 6291460

commit v7 on v6

--- a/solution.py
+++ b/solution.py
@@ -133,6 +133,15 @@
 
         lax.fori_loop(first, count, body, 0)
 
+    def unrolled(count, f, step=3):
+        def some(i):
+            for k in range(step):
+                f(i * step + k)
+
+        each(count // step, some)
+        for k in range(count - count % step, count):
+            f(k)
+
     def remote(src, dst, send, recv, where):
         return pltpu.make_async_remote_copy(
             src_ref=src, dst_ref=dst, send_sem=send, recv_sem=recv, device_id=where, device_id_type=MESH
@@ -379,7 +388,7 @@
                 at, inside = source(s, h * group + i, k)
                 v["lev"][k, pl.ds(i, 1)] = jnp.where(inside, lin[s][at], far)
 
-        each(group, one)
+        unrolled(group, one)
         levels = [v["lev"][k] for k in range(picks)] + more
         top = functools.reduce(jnp.maximum, levels)
         ws = [jnp.exp(level - top) for level in levels]
@@ -420,7 +429,7 @@
             def one(i):
                 mout[s - 1, h, i] = summed(s, h, i, blocks).astype(bf16)
 
-            each(group, one)
+            unrolled(group, one)
             for copy in merged_copies(s, h):
                 copy.start()
 
@@ -474,7 +483,7 @@
             t = span // per
             to(i, (v["gated"][t, at] + v["blend"][t, at] * memory).astype(bf16))
 
-        each(group, one)
+        unrolled(group, one)
 
     def half_copy(d):
         i = d - 1

time: 91.9 us -> 91.1 us (level)
  no operation moved by 1% of the time
where the time goes in v7:
time: 91.1 us; the launch traced here: 91 us
  Pallas kernels  88.8 us (97%)
  matrix products  2.13 us (2%)
    pallas_call x1, Pallas kernels, per_device(): pl.pallas_call(functools.partial(layer_kernel, (columns, plane, parts, lo...  88.8 us
    dot_general x1, matrix products, per_device(): jnp.dot(by_rows, output_weight, preferred_element_type=f32).astype(bf16)  2.13 us

profile of v7, /device:TPU:0, one launch (start us, length us, event | category | flops | bytes accessed | tf_op | source)
XLA Modules:
  0.0 91.0 jit_solution(9719275715301551677)
XLA Ops:
  0.0 0.0 copy-start
  0.0 88.8 %layer.1 = bf16[384,512]{1,0:T(8,128)(2,1)S(1)} custom-call(s32[4,12]{1,0:T(4,128)} %bitcast.8, f32[1,2048]{1,0:T(1,128)} %bitcast.6, f32[1,2048]{1,0:T(1,128)} %bitcast.7, f32[1,256]{1,0:T(1,128)} %bitcast.9, f32[4,128]{1,0:T(4,128)} %bias_in.1, bf16[4,128,128]{2,1,0:T(8,128)(2,1)} %mix_in.1, bf16[768,2048]{1,0:T(8,128)(2,1)} %tokens.1, ...), custom_call_target="tpu_custom_call" | custom-call | tf_op jit(solution)/shard_map/layer/pallas_call | solution.py:626
  88.8 0.0 copy-done
  88.8 2.1 %convolution_convert_fusion = bf16[384,2048]{1,0:T(8,128)(2,1)} fusion(bf16[384,512]{1,0:T(8,128)(2,1)S(1)} %layer.1, bf16[512,2048]{1,0:T(8,128)(2,1)S(1)} %copy-done), kind=kOutput, calls=%fused_computation | convolution fusion | flops 806092800 | bytes 4063232 | tf_op jit(solution)/shard_map/dot_general | solution.py:652
Async XLA Ops:
  0.0 88.8 %copy-start = (bf16[512,2048]{1,0:T(8,128)(2,1)S(1)}, bf16[512,2048]{1,0:T(8,128)(2,1)}, u32[]{:S(2)}) copy-start(bf16[512,2048]{1,0:T(8,128)(2,1)} %param.29) | copy-start | bytes 6291460
